TPU v7x, 768 devices: a whole 4x8x12 slice. The times are simulated.
768 devices in a mesh: ep: 48 (over z, x), tp: 16 (over y, core).
Axes of the slice: x: 4, y: 8, z: 12, core: 2. Of those that a mesh axis runs over, the one named last changes fastest.
Arguments:
- tokens: bfloat16 [768, 2048], P('ep'), may hold values from -6 to 6
- attn_gain: bfloat16 [2048], replicated, may hold values from 0.099609375 to 1.8984375
- ffn_gain: bfloat16 [2048], replicated, may hold values from 0.099609375 to 1.8984375
- w_query: bfloat16 [2048, 2048], P(None, 'tp'), may hold values from -0.125 to 0.125
- w_key: bfloat16 [2048, 256], replicated, may hold values from -0.125 to 0.125
- w_value: bfloat16 [2048, 256], replicated, may hold values from -0.125 to 0.125
- w_forget: bfloat16 [2048, 32], replicated, may hold values from -0.125 to 0.125
- forget_bias: float32 [32], replicated, may hold values from -1 to 3
- w_out: bfloat16 [2048, 2048], P(None, 'tp'), may hold values from -0.375 to 0.375
- cache_keys: bfloat16 [768, 2048, 256], P(('ep', 'tp')), may hold values from -800 to 800
- cache_values: bfloat16 [768, 2048, 256], P(('ep', 'tp')), may hold values from -6 to 6
- cache_logcum: float32 [768, 32, 2048], P(('ep', 'tp')), as said below
- cache_len: int32 [768], P(('ep', 'tp')), may hold values from 256 to 2048
- route_group: int32 [768], P('ep'), may hold values from 0 to 3, as said below
- route_expert: int32 [768, 2], P('ep'), may hold values from 0 to 11, as said below
- route_weight: float32 [768, 2], P('ep'), may hold values from 0.2 to 1
- w_gate: bfloat16 [48, 2048, 2048], P('ep', None, 'tp'), may hold values from -0.125 to 0.125
- w_up: bfloat16 [48, 2048, 2048], P('ep', None, 'tp'), may hold values from -0.125 to 0.125
- w_down: bfloat16 [48, 2048, 2048], P('ep', None, 'tp'), may hold values from -0.125 to 0.125
Outputs:
- layer_out: bfloat16 [768, 2048], P('ep', 'tp')
Inputs may be any that keep to these rules, and one draw needn't show every extreme that they name: Expert groups. Among the 16 sequences of one index of ep no expert route_group * 12 + route_expert is named more than 2 times, and in every draw one expert is named exactly 2 times by the sequences of every index of ep. `route_expert`: the 2 numbers of a sequence differ. `cache_logcum`: each entry is the sum of the log forget gates of that head from the first cached position up to and including that position.
All inputs are finite; a program needn't handle non-finite values.
Results may differ from a plain program's by a relative error of at most 0.012.
The roundings to bfloat16 on the way count: a program that leaves them out, or rounds other values in their place, can miss the bound.
Values may be sent and summed in bfloat16 or wider, within the bound.
No kernel may reach another device: no remote copies, remote signals or barrier semaphores. Data moves between devices by JAX's collectives and lax.ppermute only.
A program may use at most 32 MiB of HBM per device.

v0:
```python
import jax
import jax.numpy as jnp
from jax import lax
from jax.sharding import PartitionSpec as P

QUERY_HEAD_COUNT = 32
KV_HEADS = 4
HEAD = 64
GROUPS = 4
TOP = 2


NORM_EPSILON = 1e-06
MASKED_SCORE = -1e30


def copy_for_each(value, axis):
    length = lax.axis_size(axis)
    return lax.all_to_all(
        jnp.broadcast_to(value[None], (length, *value.shape)), axis, 0, 0, tiled=True
    )


def laid_out(pieces, dim):
    shape = list(pieces.shape[1:])
    shape[dim] *= pieces.shape[0]
    return jnp.moveaxis(pieces, 0, dim).reshape(shape)


def collect(value, axis, dim):
    pieces = copy_for_each(value, axis)
    return laid_out(pieces, dim)


def normalize(values, gain_vec):
    return (
        values
        * lax.rsqrt(jnp.mean(values * values, axis=-1, keepdims=True) + NORM_EPSILON)
        * gain_vec.astype(jnp.float32)
    )


def attend(query, key_new, value_new, log_gate, keys, cached_values, logcum, lengths):
    count_of_rows = query.shape[0]
    length = keys.shape[1]
    per_kv = QUERY_HEAD_COUNT // KV_HEADS
    score_scale = HEAD ** (-0.5)
    query_half = query.reshape(count_of_rows, KV_HEADS, per_kv, HEAD)
    keys_h = keys.reshape(count_of_rows, length, KV_HEADS, HEAD)
    scores = jnp.einsum("bkgd,blkd->bkgl", query_half, keys_h, preferred_element_type=jnp.float32)
    scores = scores.reshape(count_of_rows, QUERY_HEAD_COUNT, length) * score_scale
    latest = jnp.take_along_axis(logcum, (lengths - 1)[:, None, None], axis=2)
    scores = scores + latest + log_gate[:, :, None] - logcum
    usable = jnp.arange(length, dtype=jnp.int32)[None, None, :] < lengths[:, None, None]
    scores = jnp.where(usable, scores, MASKED_SCORE)
    current_key = key_new.reshape(count_of_rows, KV_HEADS, HEAD)
    current_score = jnp.einsum(
        "cnpx,cnx->cnp", query_half, current_key, preferred_element_type=jnp.float32
    )
    current_score = current_score.reshape(count_of_rows, QUERY_HEAD_COUNT) * score_scale
    peak = jnp.maximum(jnp.max(scores, axis=2), current_score)
    weights = jnp.where(usable, jnp.exp(scores - peak[:, :, None]), 0.0)
    own_weight = jnp.exp(current_score - peak)
    denominator = jnp.sum(weights, axis=2) + own_weight
    weights_b = weights.astype(jnp.bfloat16).reshape(count_of_rows, KV_HEADS, per_kv, length)
    own_b = (
        own_weight.astype(jnp.bfloat16).astype(jnp.float32).reshape(count_of_rows, KV_HEADS, per_kv)
    )
    values_h = cached_values.reshape(count_of_rows, length, KV_HEADS, HEAD)
    summed = jnp.einsum("bkgl,blkd->bkgd", weights_b, values_h, preferred_element_type=jnp.float32)
    own_value = value_new.astype(jnp.float32).reshape(count_of_rows, KV_HEADS, 1, HEAD)
    summed = summed + own_b[..., None] * own_value
    summed = summed.reshape(count_of_rows, QUERY_HEAD_COUNT, HEAD) / denominator[:, :, None]
    return summed.reshape(count_of_rows, QUERY_HEAD_COUNT * HEAD).astype(jnp.bfloat16)


def on_device(
    tokens,
    attn_gain,
    ffn_gain,
    w_query,
    w_key,
    w_value,
    w_forget,
    forget_bias,
    w_out,
    cache_keys,
    cache_values,
    cache_logcum,
    cache_len,
    route_group,
    route_expert,
    route_weight,
    w_gate,
    w_up,
    w_down,
):
    tp_index = lax.axis_index("tp")
    expert_count = lax.axis_size("ep")
    group_rows = tokens.shape[0]
    own_rows = cache_len.shape[0]
    width_part = w_out.shape[1]
    stream = tokens.astype(jnp.float32)
    normed = normalize(stream, attn_gain).astype(jnp.bfloat16)
    query_part = jnp.dot(normed, w_query, preferred_element_type=jnp.float32).astype(jnp.bfloat16)
    query = lax.all_to_all(query_part, "tp", split_axis=0, concat_axis=1, tiled=True)
    own_normed = lax.dynamic_slice_in_dim(normed, tp_index * own_rows, own_rows, 0)
    key_new = jnp.dot(own_normed, w_key, preferred_element_type=jnp.float32).astype(jnp.bfloat16)
    value_new = jnp.dot(own_normed, w_value, preferred_element_type=jnp.float32).astype(
        jnp.bfloat16
    )
    log_gate = jax.nn.log_sigmoid(
        jnp.dot(own_normed, w_forget, preferred_element_type=jnp.float32) + forget_bias
    )
    attended = attend(
        query, key_new, value_new, log_gate, cache_keys, cache_values, cache_logcum, cache_len
    )
    projected = jnp.dot(collect(attended, "tp", 0), w_out, preferred_element_type=jnp.float32)
    residual = lax.dynamic_slice_in_dim(stream, tp_index * width_part, width_part, 1)
    mixed = (residual + projected).astype(jnp.bfloat16)
    per_group = expert_count // GROUPS
    capacity = max(2, (group_rows + per_group // 2 - 1) // per_group + 1)
    picked_ids = (route_group[:, None] * per_group + route_expert).reshape(-1)
    chosen = (picked_ids[:, None] == jnp.arange(expert_count, dtype=jnp.int32)[None, :]).astype(
        jnp.int32
    )
    earlier = jnp.cumsum(chosen, axis=0) - chosen
    slot_index = jnp.sum(earlier * chosen, axis=1)
    target = picked_ids * capacity + slot_index
    place_table = (
        target[:, None] == jnp.arange(expert_count * capacity, dtype=jnp.int32)[None, :]
    ).astype(jnp.float32)
    place_table = place_table.reshape(group_rows, TOP, expert_count * capacity)
    send_table = jnp.sum(place_table, axis=1).astype(jnp.bfloat16)
    combine = jnp.sum(route_weight[:, :, None] * place_table, axis=1)
    packed = jnp.einsum("sp,sd->pd", send_table, mixed, preferred_element_type=jnp.float32).astype(
        jnp.bfloat16
    )
    full_rows = lax.all_gather(
        lax.all_to_all(
            packed.reshape(expert_count, capacity, mixed.shape[1]),
            "ep",
            split_axis=0,
            concat_axis=0,
            tiled=True,
        ),
        "tp",
        axis=2,
        tiled=True,
    )
    sources, slot_count, row_width = full_rows.shape
    flat_rows = full_rows.reshape(sources * slot_count, row_width)
    inputs = normalize(flat_rows.astype(jnp.float32), ffn_gain).astype(jnp.bfloat16)
    gate_proj = jnp.dot(inputs, w_gate[0], preferred_element_type=jnp.float32)
    up_proj = jnp.dot(inputs, w_up[0], preferred_element_type=jnp.float32)
    hidden = (jax.nn.silu(gate_proj) * up_proj).astype(jnp.bfloat16)
    rows_down = w_down[0]
    summed = jnp.dot(
        lax.all_gather(hidden, "tp", axis=1, tiled=True),
        rows_down,
        preferred_element_type=jnp.float32,
    )
    returned = summed.astype(jnp.bfloat16).reshape(sources, slot_count, w_down.shape[2])
    returned_rows = lax.all_to_all(returned, "ep", split_axis=0, concat_axis=0, tiled=True)
    moe_sum = jnp.dot(
        combine,
        returned_rows.reshape(-1, width_part).astype(jnp.float32),
        precision=lax.Precision.HIGHEST,
    )
    return (mixed.astype(jnp.float32) + moe_sum).astype(jnp.bfloat16)


def solution(mesh):
    placed = (
        P("ep", None),
        P(),
        P(),
        P(None, "tp"),
        P(),
        P(),
        P(),
        P(),
        P(None, "tp"),
        P(("ep", "tp"), None, None),
        P(("ep", "tp"), None, None),
        P(("ep", "tp"), None, None),
        P(("ep", "tp")),
        P("ep"),
        P("ep", None),
        P("ep", None),
        P("ep", None, "tp"),
        P("ep", None, "tp"),
        P("ep", None, "tp"),
    )
    return jax.shard_map(
        on_device, mesh=mesh, in_specs=placed, out_specs=P("ep", "tp"), check_vma=False
    )
```

profile of v0, /device:TPU:1, one launch (start us, length us, event | category | flops | bytes accessed | tf_op | source)
XLA Modules:
  0.0 123.1 jit_solution(4986807858427267003)
XLA Ops:
  0.0 0.8 convert_element_type.94
  0.9 1.0 multiply_reduce_fusion
  1.9 1.2 fusion.8
  3.1 0.6 copy.49
  3.8 13.8 %all-to-all-start = ((bf16[16,1,128]{2,1,0:T(2,128)(2,1)}), bf16[16,1,128]{2,1,0:T(2,128)(2,1)S(1)}, u32[]{:S(2)}, u32[]{:S(2)}) async-start(bf16[16,1,128]{2,1,0:T(2,128)(2,1)} %copy.49), calls=%async_computation | async-start | bytes 16384 | tf_op jit(solution)/shard_map/all_to_all | solution.py:106
  18.7 0.7 copy-done.10
  19.4 0.6 copy-done.12
  20.5 0.5 copy-done.11
  21.2 1.5 %copy.50 = bf16[1,2048,256]{1,2,0:T(8,128)(2,1)S(1)} copy(bf16[1,2048,256]{2,1,0:T(8,128)(2,1)} %param.28) | data formatting | bytes 2097152 | tf_op args[9]
  22.8 1.5 %copy.51 = bf16[1,2048,256]{1,2,0:T(8,128)(2,1)S(1)} copy(bf16[1,2048,256]{2,1,0:T(8,128)(2,1)} %param.29) | data formatting | bytes 2097152 | tf_op args[10]
  24.4 0.9 select_reduce_fusion
  25.5 1.3 %fusion.41 = (f32[32]{0:T(128)S(1)}, f32[1,32,2048]{2,1,0:T(8,128)S(1)}) fusion(f32[1,32,2048]{2,1,0:T(8,128)} %param.30, f32[32]{0:T(128)S(1)} %fusion.37, f32[32]{0:T(128)S(1)} %select_reduce_fusion, bf16[4,8,64]{2,1,0:T(8,128)(2,1)S(1)} %reshape.324, bf16[2048,4,64]{0,2,1:T(8,128)(2,1)S(1)} %bitcast.77, pred[2048]{0:T(1024)(128)(4,1)S(1)} %iota_compare_fusion.2), kind=kOutput, calls=%fused_computation.72 | convolution fusion | flops 8781792 | bytes 1579392 | tf_op jit(solution)/shard_map/bkgd,blkd->bkgl/dot_general | solution.py:50
  27.5 0.4 convolution_add_fusion
  28.1 0.5 broadcast.205
  28.7 1.0 reduce.10
  29.7 0.7 reshape.397
  30.3 7.3 %all-to-all-start.1 = ((bf16[16,2,1024]{2,1,0:T(2,128)(2,1)}), bf16[16,2,1024]{2,1,0:T(2,128)(2,1)S(1)}, u32[]{:S(2)}, u32[]{:S(2)}) async-start(bf16[16,2,1024]{2,1,0:T(2,128)(2,1)} %reshape.397), calls=%async_computation.1 | async-start | bytes 131072 | tf_op jit(solution)/shard_map/all_to_all | solution.py:19
  37.8 0.7 copy-done.9
  38.5 6.8 %all-to-all-done.1 = bf16[16,2,1024]{2,1,0:T(2,128)(2,1)S(1)} async-done(((bf16[16,2,1024]{2,1,0:T(2,128)(2,1)}), bf16[16,2,1024]{2,1,0:T(2,128)(2,1)S(1)}, u32[]{:S(2)}, u32[]{:S(2)}) %all-to-all-start.1) | async-done | bytes 65568 | tf_op jit(solution)/shard_map/all_to_all | solution.py:19
  45.6 0.8 convolution_convert_fusion.1
  46.4 13.0 %all-to-all-start.2 = ((bf16[48,2,128]{2,1,0:T(2,128)(2,1)}), bf16[48,2,128]{2,1,0:T(2,128)(2,1)S(1)}, u32[]{:S(2)}, u32[]{:S(2)}) async-start(bf16[48,2,128]{2,1,0:T(2,128)(2,1)} %bitcast.14), calls=%async_computation.2 | async-start | bytes 49152 | tf_op jit(solution)/shard_map/all_to_all | solution.py:140
  59.4 10.9 %all-to-all-done.2 = bf16[48,2,128]{2,1,0:T(2,128)(2,1)S(1)} async-done(((bf16[48,2,128]{2,1,0:T(2,128)(2,1)}), bf16[48,2,128]{2,1,0:T(2,128)(2,1)S(1)}, u32[]{:S(2)}, u32[]{:S(2)}) %all-to-all-start.2) | async-done | bytes 24608 | tf_op jit(solution)/shard_map/all_to_all | solution.py:140
  70.2 17.2 %all_gather.6 = bf16[48,2,2048]{2,1,0:T(2,128)(2,1)S(1)} all-gather(bf16[48,2,128]{2,1,0:T(2,128)(2,1)S(1)} %all-to-all-done.2), channel_id=1, replica_groups=mesh['ep'=48,'tp'=16] {'tp'}, dimensions={2}, use_global_device_ids=true | all-gather | bytes 417792 | tf_op jit(solution)/shard_map/all_gather | solution.py:139
  87.5 0.5 fusion.11
  88.0 0.5 fusion.13
  88.6 0.9 copy-done.5
  89.8 0.8 copy-done.6
  90.6 0.3 fusion.5
  90.8 16.5 %all_gather.7 = bf16[96,2048]{1,0:T(8,128)(2,1)S(1)} all-gather(bf16[96,128]{1,0:T(8,128)(2,1)S(1)} %fusion.5), channel_id=1, replica_groups=mesh['ep'=48,'tp'=16] {'tp'}, dimensions={1}, use_global_device_ids=true | all-gather | bytes 417792 | tf_op jit(solution)/shard_map/all_gather | solution.py:159
  107.4 0.3 convolution_convert_fusion
  107.6 14.7 %all_to_all.28 = bf16[48,2,128]{2,1,0:T(2,128)(2,1)S(1)} all-to-all(bf16[48,2,128]{2,1,0:T(2,128)(2,1)S(1)} %bitcast.79), channel_id=1, replica_groups=mesh['ep'=48,'tp'=16] {'ep'}, dimensions={0} | all-to-all | bytes 49152 | tf_op jit(solution)/shard_map/all_to_all | solution.py:164
  122.3 0.7 fusion.6
  (63 shorter events, 3.5 us)
Async XLA Ops:
  0.0 18.2 %copy-start = (bf16[2048,256]{1,0:T(8,128)(2,1)S(1)}, bf16[2048,256]{1,0:T(8,128)(2,1)}, u32[]{:S(2)}) copy-start(bf16[2048,256]{1,0:T(8,128)(2,1)} %param.23) | copy-start | bytes 3145732
  0.0 1.8 %copy-start.2 = (bf16[16,2048]{1,0:T(8,128)(2,1)S(1)}, bf16[16,2048]{1,0:T(8,128)(2,1)}, u32[]{:S(2)}) copy-start(bf16[16,2048]{1,0:T(8,128)(2,1)} %param.19) | copy-start | bytes 196612
  0.0 18.4 %copy-start.1 = (bf16[2048,256]{1,0:T(8,128)(2,1)S(1)}, bf16[2048,256]{1,0:T(8,128)(2,1)}, u32[]{:S(2)}) copy-start(bf16[2048,256]{1,0:T(8,128)(2,1)} %param.24) | copy-start | bytes 3145732
  3.8 21.6 %all-to-all-start = ((bf16[16,1,128]{2,1,0:T(2,128)(2,1)}), bf16[16,1,128]{2,1,0:T(2,128)(2,1)S(1)}, u32[]{:S(2)}, u32[]{:S(2)}) async-start(bf16[16,1,128]{2,1,0:T(2,128)(2,1)} %copy.49), calls=%async_computation | async-start | bytes 16384 | tf_op jit(solution)/shard_map/all_to_all | solution.py:106
  18.4 2.1 %copy-start.7 = (bf16[2048,32]{0,1:T(8,128)(2,1)S(1)}, bf16[2048,32]{0,1:T(8,128)(2,1)}, u32[]{:S(2)}) copy-start(bf16[2048,32]{0,1:T(8,128)(2,1)} %param.25) | copy-start | bytes 393220
  18.7 0.7 copy-start.10
  19.4 0.7 copy-start.12
  20.3 0.7 copy-start.11
  28.0 17.4 %copy-start.4 = (bf16[2048,128]{1,0:T(8,128)(2,1)S(1)}, bf16[2048,128]{1,0:T(8,128)(2,1)}, u32[]{:S(2)}) copy-start(bf16[2048,128]{1,0:T(8,128)(2,1)} %param.27) | copy-start | bytes 1572868
  30.3 15.0 %all-to-all-start.1 = ((bf16[16,2,1024]{2,1,0:T(2,128)(2,1)}), bf16[16,2,1024]{2,1,0:T(2,128)(2,1)S(1)}, u32[]{:S(2)}, u32[]{:S(2)}) async-start(bf16[16,2,1024]{2,1,0:T(2,128)(2,1)} %reshape.397), calls=%async_computation.1 | async-start | bytes 131072 | tf_op jit(solution)/shard_map/all_to_all | solution.py:19
  37.8 0.7 copy-start.9
  46.4 13.0 %copy-start.8 = (bf16[2048]{0:T(1024)(128)(2,1)S(1)}, bf16[2048]{0:T(1024)(128)(2,1)}, u32[]{:S(2)}) copy-start(bf16[2048]{0:T(1024)(128)(2,1)} %param.21) | copy-start | bytes 12292
  46.4 23.8 %all-to-all-start.2 = ((bf16[48,2,128]{2,1,0:T(2,128)(2,1)}), bf16[48,2,128]{2,1,0:T(2,128)(2,1)S(1)}, u32[]{:S(2)}, u32[]{:S(2)}) async-start(bf16[48,2,128]{2,1,0:T(2,128)(2,1)} %bitcast.14), calls=%async_computation.2 | async-start | bytes 49152 | tf_op jit(solution)/shard_map/all_to_all | solution.py:140
  88.5 1.0 copy-start.5
  89.5 1.0 copy-start.6
  90.6 16.8 %copy-start.3 = (bf16[1,2048,128]{2,1,0:T(8,128)(2,1)S(1)}, bf16[1,2048,128]{2,1,0:T(8,128)(2,1)}, u32[]{:S(2)}) copy-start(bf16[1,2048,128]{2,1,0:T(8,128)(2,1)} %param.37) | copy-start | bytes 1572868
where the time goes:
time: 124 us; the launch traced here: 123 us
  blocking collectives  48.5 us (39%)
  starting transfers between devices  34 us (27%)
  waiting for transfers between devices  17.7 us (14%)
  local copies, waits for them, and re-layouts  10.1 us (8%)
  matrix products  6.23 us (5%)
  other arithmetic  5.65 us (5%)
    all_gather x1, blocking collectives, on_device(): lax.all_gather(lax.all_to_all(packed.reshape(expert_count, capacity, mixe...  17.2 us
    all_gather x1, blocking collectives, on_device(): lax.all_gather(hidden, 'tp', axis=1, tiled=True)  16.5 us
    all_to_all x1, blocking collectives, on_device(): lax.all_to_all(returned, 'ep', split_axis=0, concat_axis=0, tiled=True)  14.7 us
    all_to_all x1, starting transfers between devices, on_device(): lax.all_to_all(query_part, 'tp', split_axis=0, concat_axis=1, tiled=True)  13.8 us
    all_to_all x1, starting transfers between devices, on_device(): lax.all_to_all(packed.reshape(expert_count, capacity, mixed.shape[1]), 'e...  13 us
    all_to_all x1, waiting for transfers between devices, on_device(): lax.all_to_all(packed.reshape(expert_count, capacity, mixed.shape[1]), 'e...  10.9 us
    unnamed x31, local copies, waits for them, and re-layouts  7.85 us
    all_to_all x1, starting transfers between devices, copy_for_each(): lax.all_to_all(jnp.broadcast_to(value[None], (length, *value.shape)), axi...  7.27 us
  transfers between devices with their start and end apart: 3, of which 2 were waited for; matrix products, arithmetic and copies ran while one was open for 5% of the time, Pallas kernels for 0%

commit v1 on v0

v1 whole, which is shorter than its diff:
```python
import jax
import jax.numpy as jnp
from jax import lax
from jax.experimental import pallas as pl
from jax.experimental.pallas import tpu as pltpu
from jax.sharding import Mesh
from jax.sharding import PartitionSpec as P

QUERY_HEAD_COUNT = 32
KV_HEADS = 4
HEAD = 64
GROUPS = 4
TOP = 2
NORM_EPSILON = 1e-06
MASKED_SCORE = -1e30
CORES = 2
VMEM_LIMIT = 8 * 1024 * 1024

F32 = jnp.float32
BF16 = jnp.bfloat16
VM = pl.BlockSpec(memory_space=pltpu.VMEM)
SM = pl.BlockSpec(memory_space=pltpu.SMEM)


def call(body, outs, operands, specs, scratch=(), flops=1_000_000, moved=1_000_000):
    return pl.pallas_call(
        body,
        out_shape=outs,
        in_specs=specs,
        out_specs=jax.tree.map(lambda _: VM, outs),
        scratch_shapes=list(scratch),
        compiler_params=pltpu.CompilerParams(vmem_limit_bytes=VMEM_LIMIT),
        cost_estimate=pl.CostEstimate(flops=flops, bytes_accessed=moved, transcendentals=0),
    )(*operands)


def shaped(shape, dtype):
    return jax.ShapeDtypeStruct(shape, dtype)


def query_kernel(tokens_ref, gain_ref, w_ref, normed_ref, query_ref):
    values = tokens_ref[...].astype(F32)
    mean = jnp.mean(values * values, axis=-1, keepdims=True)
    scaled = values * lax.rsqrt(mean + NORM_EPSILON)
    lanes = gain_ref.shape[1]
    normed = jnp.concatenate(
        [
            (scaled[:, i * lanes : (i + 1) * lanes] * gain_ref[i : i + 1].astype(F32)).astype(BF16)
            for i in range(gain_ref.shape[0])
        ],
        axis=1,
    )
    normed_ref[...] = normed
    query_ref[...] = jnp.dot(normed, w_ref[...], preferred_element_type=F32).astype(BF16)


def side_kernel(
    place_ref,
    normed_ref,
    w_key_ref,
    w_value_ref,
    w_forget_ref,
    bias_ref,
    group_ref,
    expert_ref,
    weight_ref,
    key_ref,
    value_ref,
    gate_ref,
    send_ref,
    combine_ref,
    *,
    per_group,
):
    place = place_ref[0]
    normed = normed_ref[...]
    rows = normed.shape[0]
    own_row = lax.broadcasted_iota(jnp.int32, (rows, 1), 0) == place

    def projected(w_ref):
        full = jnp.dot(normed, w_ref[...], preferred_element_type=F32)
        return jnp.sum(jnp.where(own_row, full, 0.0), axis=0, keepdims=True)

    key_ref[...] = projected(w_key_ref).astype(BF16).astype(F32)
    value_ref[...] = projected(w_value_ref).astype(BF16).astype(F32)
    logits = lax.dot_general(
        w_forget_ref[...], normed, (((1,), (1,)), ((), ())), preferred_element_type=F32
    )
    heads = logits.shape[0]
    own_column = lax.broadcasted_iota(jnp.int32, (1, rows), 1) == place
    logit = jnp.sum(jnp.where(own_column, logits, 0.0), axis=1, keepdims=True)
    diagonal = lax.broadcasted_iota(jnp.int32, (heads, heads), 0) == lax.broadcasted_iota(
        jnp.int32, (heads, heads), 1
    )
    bias = jnp.sum(jnp.where(diagonal, bias_ref[...], 0.0), axis=1, keepdims=True)
    logit = logit + bias
    log_gate = jnp.minimum(logit, 0.0) - jnp.log1p(jnp.exp(-jnp.abs(logit)))
    gate_ref[...] = jnp.broadcast_to(log_gate, gate_ref.shape)

    picked = group_ref[...] * per_group + expert_ref[...]
    row_index = lax.broadcasted_iota(jnp.int32, (rows, rows), 0)
    column_index = lax.broadcasted_iota(jnp.int32, (rows, rows), 1)
    lines = [picked[j : j + 1] for j in range(TOP)]
    columns = [
        jnp.sum(jnp.where(row_index == column_index, line, 0), axis=1, keepdims=True)
        for line in lines
    ]
    slots, _ = send_ref.shape
    slot_index = lax.broadcasted_iota(jnp.int32, (slots, rows), 0)
    send = jnp.zeros((slots, rows), F32)
    combine = jnp.zeros((slots, rows), F32)
    for j in range(TOP):
        earlier = jnp.zeros((1, rows), jnp.int32)
        for other in columns:
            same = (other == lines[j]) & (row_index < column_index)
            earlier = earlier + jnp.sum(same.astype(jnp.int32), axis=0, keepdims=True)
        hit = slot_index == lines[j] * TOP + earlier
        send = send + jnp.where(hit, 1.0, 0.0)
        combine = combine + jnp.where(hit, weight_ref[j : j + 1], 0.0)
    send_ref[...] = send.astype(BF16)
    combine_ref[...] = combine


def attend_kernel(
    length_ref, query_ref, key_new_ref, value_new_ref, gate_ref, keys_ref, values_ref, cum_ref, out_ref
):
    heads = QUERY_HEAD_COUNT
    pairs = heads // 2
    width = KV_HEADS * HEAD
    used = length_ref[0]

    def index(shape, dim):
        return lax.broadcasted_iota(jnp.int32, shape, dim)

    to_heads = (index((heads, pairs), 0) // 2 == index((heads, pairs), 1)).astype(BF16)
    to_pairs = (index((pairs, heads), 1) // 2 == index((pairs, heads), 0)).astype(BF16)
    doubled = jnp.dot(to_heads, query_ref[...], preferred_element_type=F32)
    odd_row = index((heads, HEAD), 0) % 2 == 1
    one_head = jnp.where(odd_row, doubled[:, HEAD:], doubled[:, :HEAD])
    in_block = index((heads, width), 1) // HEAD == index((heads, width), 0) // (heads // KV_HEADS)
    query_wide = jnp.where(in_block, jnp.concatenate([one_head] * KV_HEADS, axis=1), 0.0)
    query_all = query_wide.astype(BF16)
    scores = lax.dot_general(
        query_all, keys_ref[0], (((1,), (1,)), ((), ())), preferred_element_type=F32
    )
    cum = cum_ref[0]
    log_gate = gate_ref[:, :1]
    position = lax.broadcasted_iota(jnp.int32, scores.shape, 1)
    latest = jnp.sum(jnp.where(position == used - 1, cum, 0.0), axis=1, keepdims=True)
    scores = scores * (HEAD**-0.5) + latest + log_gate - cum
    usable = position < used
    scores = jnp.where(usable, scores, MASKED_SCORE)
    own = jnp.sum(query_wide * key_new_ref[...], axis=1, keepdims=True) * (HEAD**-0.5)
    peak = jnp.maximum(jnp.max(scores, axis=1, keepdims=True), own)
    weights = jnp.where(usable, jnp.exp(scores - peak), 0.0)
    own_weight = jnp.exp(own - peak)
    denominator = jnp.sum(weights, axis=1, keepdims=True) + own_weight
    summed = jnp.dot(weights.astype(BF16), values_ref[0], preferred_element_type=F32)
    summed = summed + own_weight.astype(BF16).astype(F32) * value_new_ref[...]
    summed = jnp.where(in_block, summed, 0.0)
    summed = summed[:, : 2 * HEAD] + summed[:, 2 * HEAD :]
    summed = (summed[:, :HEAD] + summed[:, HEAD:]) / denominator
    both = jnp.concatenate([summed, summed], axis=1).astype(BF16)
    mine = index(both.shape, 1) // HEAD == index(both.shape, 0) % 2
    both = jnp.where(mine, both, jnp.zeros((), BF16))
    attended = jnp.dot(to_pairs, both, preferred_element_type=F32).astype(BF16)
    out_ref[...] = jnp.broadcast_to(attended[None], out_ref.shape)


def mix_kernel(place_ref, parts_ref, w_ref, tokens_ref, send_ref, mixed_ref, packed_ref, wide_ref):
    rows, chunks, lanes = parts_ref.shape
    wide_ref[...] = parts_ref[...].reshape(rows * chunks, lanes).astype(F32)
    attended = jnp.concatenate(
        [wide_ref[pl.ds(i, rows, stride=chunks), :].astype(BF16) for i in range(chunks)], axis=1
    )
    projected = jnp.dot(attended, w_ref[...], preferred_element_type=F32)
    first = pl.multiple_of(place_ref[0] * lanes, lanes)
    residual = tokens_ref[:, pl.ds(first, lanes)].astype(F32)
    mixed = (residual + projected).astype(BF16)
    mixed_ref[...] = mixed
    packed_ref[...] = jnp.dot(send_ref[...], mixed, preferred_element_type=F32).astype(BF16)


def hidden_kernel(parts_ref, gain_ref, w_gate_ref, w_up_ref, out_ref, inputs_ref):
    cores, chips, rows, lanes = parts_ref.shape
    squares = jnp.zeros((rows, lanes), F32)
    for core in range(cores):
        for chip in range(chips):
            part = parts_ref[core, chip].astype(F32)
            squares = squares + part * part
    mean = jnp.sum(squares, axis=-1, keepdims=True) / (cores * chips * lanes)
    scale = lax.rsqrt(mean + NORM_EPSILON)
    for core in range(cores):
        for chip in range(chips):
            first = (chip * cores + core) * lanes
            part = parts_ref[core, chip].astype(F32)
            gain = gain_ref[chip * cores + core : chip * cores + core + 1].astype(F32)
            inputs_ref[:, first : first + lanes] = (part * scale * gain).astype(BF16)
    inputs = inputs_ref[...]
    gate = jnp.dot(inputs, w_gate_ref[0], preferred_element_type=F32)
    up = jnp.dot(inputs, w_up_ref[0], preferred_element_type=F32)
    hidden = (gate / (1.0 + jnp.exp(-gate)) * up).astype(BF16)
    out_ref[...] = jnp.broadcast_to(hidden[None], out_ref.shape)


def down_kernel(parts_ref, w_ref, out_ref, hidden_ref):
    cores, chips, _, lanes = parts_ref.shape
    for core in range(cores):
        for chip in range(chips):
            first = (chip * cores + core) * lanes
            hidden_ref[:, first : first + lanes] = parts_ref[core, chip]
    out_ref[...] = jnp.dot(hidden_ref[...], w_ref[0], preferred_element_type=F32).astype(BF16)


def combine_kernel(returned_ref, combine_ref, mixed_ref, out_ref):
    returned = returned_ref[...]
    rest = combine_ref[...]
    total = jnp.zeros(out_ref.shape, F32)
    for _ in range(3):
        part = rest.astype(BF16)
        rest = rest - part.astype(F32)
        total = total + lax.dot_general(
            part, returned, (((0,), (0,)), ((), ())), preferred_element_type=F32
        )
    out_ref[...] = (mixed_ref[...].astype(F32) + total).astype(BF16)


def solution(mesh):
    experts = mesh.shape["ep"]
    peers = mesh.shape["tp"]
    chips = peers // CORES
    split = Mesh(mesh.devices.reshape(experts, chips, CORES), ("ep", "y", "core"))
    tp = ("y", "core")

    def to_all(copies):
        exchanged = lax.all_to_all(copies, "y", 0, 0, tiled=True)
        return lax.all_gather(exchanged, "core", axis=0, tiled=False)

    def on_device(
        tokens,
        attn_gain,
        ffn_gain,
        w_query,
        w_key,
        w_value,
        w_forget,
        forget_bias,
        w_out,
        cache_keys,
        cache_values,
        cache_logcum,
        cache_len,
        route_group,
        route_expert,
        route_weight,
        w_gate,
        w_up,
        w_down,
    ):
        rows, features = tokens.shape
        part = w_query.shape[1]
        slots = experts * TOP
        place = (lax.axis_index("y") * CORES + lax.axis_index("core")).astype(jnp.int32)
        place = place.reshape(1)
        normed, query = call(
            query_kernel,
            (shaped((rows, features), BF16), shaped((rows, part), BF16)),
            (tokens, attn_gain.reshape(peers, part), w_query),
            [VM] * 3,
            flops=20_000_000,
        )
        own_query = lax.all_to_all(
            query.reshape(peers, 1, part), tp, split_axis=0, concat_axis=0, tiled=True
        ).reshape(peers, part)

        def side(*refs):
            side_kernel(*refs, per_group=experts // GROUPS)

        kv = w_key.shape[1]
        key_new, value_new, log_gate, send, combine = call(
            side,
            (
                shaped((1, kv), F32),
                shaped((1, kv), F32),
                shaped((QUERY_HEAD_COUNT, 128), F32),
                shaped((slots, rows), BF16),
                shaped((slots, rows), F32),
            ),
            (
                place,
                normed,
                w_key,
                w_value,
                w_forget.T,
                forget_bias.reshape(1, QUERY_HEAD_COUNT),
                route_group.reshape(1, rows),
                route_expert.T,
                route_weight.T,
            ),
            [SM] + [VM] * 8,
            flops=2_000_000_000,
        )
        copies = call(
            attend_kernel,
            shaped((peers, peers, part), BF16),
            (cache_len, own_query, key_new, value_new, log_gate, cache_keys, cache_values, cache_logcum),
            [SM] + [VM] * 7,
            flops=200_000_000,
        )
        attended = lax.all_to_all(copies, tp, 0, 0, tiled=True)
        mixed, packed = call(
            mix_kernel,
            (shaped((rows, part), BF16), shaped((slots, part), BF16)),
            (place, attended, w_out, tokens, send),
            [SM] + [VM] * 4,
            scratch=[pltpu.VMEM((rows * peers, part), F32)],
            flops=20_000_000,
        )
        arrived = lax.all_to_all(packed.reshape(experts, TOP, part), "ep", 0, 0, tiled=True)
        arrived = arrived.reshape(slots, part)
        parts = to_all(jnp.broadcast_to(arrived[None], (chips, slots, part)))
        hidden = call(
            hidden_kernel,
            shaped((chips, slots, part), BF16),
            (parts, ffn_gain.reshape(peers, part), w_gate, w_up),
            [VM] * 4,
            scratch=[pltpu.VMEM((slots, features), BF16)],
            flops=100_000_000,
        )
        result = call(
            down_kernel,
            shaped((slots, part), BF16),
            (to_all(hidden), w_down),
            [VM] * 2,
            scratch=[pltpu.VMEM((slots, features), BF16)],
            flops=50_000_000,
        )
        returned = lax.all_to_all(result.reshape(experts, TOP, part), "ep", 0, 0, tiled=True)
        return call(
            combine_kernel,
            shaped((rows, part), BF16),
            (returned.reshape(slots, part), combine, mixed),
            [VM] * 3,
            flops=2_000_000,
        )

    placed = (
        P("ep", None),
        P(),
        P(),
        P(None, tp),
        P(),
        P(),
        P(),
        P(),
        P(None, tp),
        P(("ep", *tp), None, None),
        P(("ep", *tp), None, None),
        P(("ep", *tp), None, None),
        P(("ep", *tp)),
        P("ep"),
        P("ep", None),
        P("ep", None),
        P("ep", None, tp),
        P("ep", None, tp),
        P("ep", None, tp),
    )
    return jax.shard_map(
        on_device, mesh=split, in_specs=placed, out_specs=P("ep", tp), check_vma=False
    )
```

time: 124 us -> 111 us (0.90)
  blocking collectives: 48.5 us -> 82.4 us
  starting transfers between devices: 34 us -> 13.7 us
  waiting for transfers between devices: 17.7 us -> 2.56 us
  matrix products: 6.23 us -> 0 us
  other arithmetic: 5.65 us -> 0 us
  Pallas kernels: 0 us -> 4.13 us
  local copies, waits for them, and re-layouts: 10.1 us -> 6.38 us
    all_to_all x1 -> x5, blocking collectives: 14.7 us -> 74.4 us  [the longest x1 23.6 us: on_device(): lax.all_to_all(packed.reshape(experts, TOP, part), 'ep', 0, 0, tiled=True)]
    all_gather x2, blocking collectives: 33.8 us -> 7.94 us  [to_all(): return lax.all_gather(exchanged, 'core', axis=0, tiled=False)]
    all_to_all x3 -> x1, starting transfers between devices: 34 us -> 13.7 us  [on_device(): lax.all_to_all(query.reshape(peers, 1, part), tp, split_axis=0, concat_ax...]
    all_to_all x3 -> x1, waiting for transfers between devices: 17.7 us -> 2.56 us  [on_device(): lax.all_to_all(query.reshape(peers, 1, part), tp, split_axis=0, concat_ax...]
    dot_general x13 -> x0, matrix products: 6.23 us -> none  [the longest x1 1.31 us: attend(): jnp.einsum('bkgd,blkd->bkgl', query_half, keys_h, preferred_element_type=...]
    pallas_call x0 -> x7, Pallas kernels: none -> 4.13 us  [call(): pl.pallas_call(body, out_shape=outs, in_specs=specs, out_specs=jax.tree.m...]
    unnamed x31 -> x39, local copies, waits for them, and re-layouts: 7.85 us -> 5.74 us
    reduce_sum x5 -> x0, other arithmetic: 1.95 us -> none  [the longest x2 1.45 us: normalize(): jnp.mean(values * values, axis=-1, keepdims=True) + NORM_EPSILON]
  transfers between devices with their start and end apart: 3 -> 1, of which waited for: 2 -> 1; matrix products, arithmetic and copies ran while one was open for 5% -> 0% of each run, Pallas kernels for 0% -> 0%
where the time goes in v1:
time: 111 us; the launch traced here: 110 us
  blocking collectives  82.4 us (74%)
  starting transfers between devices  13.7 us (12%)
  local copies, waits for them, and re-layouts  6.38 us (6%)
  Pallas kernels  4.13 us (4%)
  waiting for transfers between devices  2.56 us (2%)
    all_to_all x1, blocking collectives, on_device(): lax.all_to_all(packed.reshape(experts, TOP, part), 'ep', 0, 0, tiled=True)  23.6 us
    all_to_all x2, blocking collectives, to_all(): exchanged = lax.all_to_all(copies, 'y', 0, 0, tiled=True)  23.5 us
    all_to_all x1, blocking collectives, on_device(): lax.all_to_all(result.reshape(experts, TOP, part), 'ep', 0, 0, tiled=True)  14.7 us
    all_to_all x1, starting transfers between devices, on_device(): lax.all_to_all(query.reshape(peers, 1, part), tp, split_axis=0, concat_ax...  13.7 us
    all_to_all x1, blocking collectives, on_device(): attended = lax.all_to_all(copies, tp, 0, 0, tiled=True)  12.6 us
    all_gather x2, blocking collectives, to_all(): return lax.all_gather(exchanged, 'core', axis=0, tiled=False)  7.94 us
    unnamed x39, local copies, waits for them, and re-layouts  5.74 us
    pallas_call x7, Pallas kernels, call(): pl.pallas_call(body, out_shape=outs, in_specs=specs, out_specs=jax.tree.m...  4.13 us
  transfers between devices with their start and end apart: 1, of which 1 were waited for; matrix products, arithmetic and copies ran while one was open for 0% of the time, Pallas kernels for 0%

profile of v1, /device:TPU:1, one launch (start us, length us, event | category | flops | bytes accessed | tf_op | source)
XLA Modules:
  0.0 110.1 jit_solution(7403827551670193934)
XLA Ops:
  0.0 1.0 copy-done.5
  1.0 0.8 copy-done.8
  1.9 0.7 copy-done.10
  2.6 0.3 shard_map.181
  2.8 0.6 copy.21
  3.5 13.7 %all-to-all-start = ((bf16[16,1,128]{2,1,0:T(2,128)(2,1)}), bf16[16,1,128]{2,1,0:T(2,128)(2,1)S(1)}, u32[]{:S(2)}, u32[]{:S(2)}) async-start(bf16[16,1,128]{2,1,0:T(2,128)(2,1)} %copy.21), calls=%async_computation | async-start | bytes 16384 | tf_op jit(solution)/shard_map/all_to_all | solution.py:272
  17.2 0.0 copy-start.18
  17.2 0.0 copy-start.15
  17.2 0.0 copy-start.17
  17.2 0.0 copy-done.14
  17.3 0.6 copy-done.16
  17.9 0.0 copy-done.15
  17.9 1.2 %copy-done.12 = bf16[2048,256]{1,0:T(8,128)(2,1)S(1)} copy-done((bf16[2048,256]{1,0:T(8,128)(2,1)S(1)}, bf16[2048,256]{1,0:T(8,128)(2,1)}, u32[]{:S(2)}) %copy-start.12) | copy-done | bytes 1048600
  19.1 1.2 %copy-done.13 = bf16[2048,256]{1,0:T(8,128)(2,1)S(1)} copy-done((bf16[2048,256]{1,0:T(8,128)(2,1)S(1)}, bf16[2048,256]{1,0:T(8,128)(2,1)}, u32[]{:S(2)}) %copy-start.13) | copy-done | bytes 1048600
  20.4 0.5 shard_map.182
  21.7 2.6 %all-to-all-done = bf16[16,1,128]{2,1,0:T(2,128)(2,1)S(1)} async-done(((bf16[16,1,128]{2,1,0:T(2,128)(2,1)}), bf16[16,1,128]{2,1,0:T(2,128)(2,1)S(1)}, u32[]{:S(2)}, u32[]{:S(2)}) %all-to-all-start) | async-done | bytes 4128 | tf_op jit(solution)/shard_map/all_to_all | solution.py:272
  24.3 0.0 copy-done
  24.3 0.0 copy-start.6
  24.3 1.4 %shard_map.183 = bf16[16,16,128]{2,1,0:T(8,128)(2,1)S(1)} custom-call(s32[1]{0:T(128)S(6)} %copy.25.length_ref, bf16[16,128]{1,0:T(8,128)(2,1)S(1)} %bitcast.23, f32[1,256]{1,0:T(1,128)S(1)} %get-tuple-element.16.key_new_ref, f32[1,256]{1,0:T(1,128)S(1)} %get-tuple-element.17.value_new_ref, f32[32,128]{1,0:T(8,128)S(1)} %get-tuple-element.18.gate_ref, ...), custom_call_target="tpu_custom_call" | custom-call | flops 200000000 | bytes 1000000 | tf_op jit(solution)/shard_map/pallas_call | solution.py:26
  25.8 12.6 %all_to_all.30.parts_ref = bf16[16,16,128]{2,1,0:T(8,128)(2,1)S(1)} all-to-all(bf16[16,16,128]{2,1,0:T(8,128)(2,1)S(1)} %shard_map.183), channel_id=1, replica_groups=mesh['ep'=48,'y'=8,'core'=2] {'y','core'}, dimensions={0} | all-to-all | bytes 131072 | tf_op jit(solution)/shard_map/all_to_all | solution.py:310
  38.4 0.3 shard_map.184
  38.7 23.6 %all_to_all.31 = bf16[48,2,128]{2,1,0:T(2,128)(2,1)S(1)} all-to-all(bf16[48,2,128]{2,1,0:T(2,128)(2,1)S(1)} %bitcast.22), channel_id=1, replica_groups=mesh['ep'=48,'y'=8,'core'=2] {'ep'}, dimensions={0} | all-to-all | bytes 49152 | tf_op jit(solution)/shard_map/all_to_all | solution.py:319
  62.3 0.0 copy-start.2
  62.3 11.0 %all_to_all.32 = bf16[8,96,128]{2,1,0:T(8,128)(2,1)S(1)} all-to-all(bf16[8,96,128]{2,1,0:T(8,128)(2,1)S(1)} %broadcast_in_dim.8), channel_id=1, replica_groups=mesh['ep'=48,'y'=8,'core'=2] {'y'}, dimensions={0} | all-to-all | bytes 393216 | tf_op jit(solution)/shard_map/all_to_all | solution.py:236
  73.3 4.8 %all-gather = bf16[16,96,128]{2,1,0:T(8,128)(2,1)S(1)} all-gather(bf16[8,96,128]{2,1,0:T(8,128)(2,1)S(1)} %all_to_all.32), channel_id=2, replica_groups=mesh['ep'=48,'y'=8,'core'=2] {'core'}, dimensions={0}, use_global_device_ids=true | all-gather | bytes 589824 | tf_op jit(solution)/shard_map/all_gather | solution.py:237
  78.1 0.5 shard_map.185
  78.7 0.0 copy-start.4
  78.7 12.5 %all_to_all.33 = bf16[8,96,128]{2,1,0:T(8,128)(2,1)S(1)} all-to-all(bf16[8,96,128]{2,1,0:T(8,128)(2,1)S(1)} %shard_map.185), channel_id=1, replica_groups=mesh['ep'=48,'y'=8,'core'=2] {'y'}, dimensions={0} | all-to-all | bytes 393216 | tf_op jit(solution)/shard_map/all_to_all | solution.py:236
  91.2 3.1 %all-gather.1 = bf16[16,96,128]{2,1,0:T(8,128)(2,1)S(1)} all-gather(bf16[8,96,128]{2,1,0:T(8,128)(2,1)S(1)} %all_to_all.33), channel_id=3, replica_groups=mesh['ep'=48,'y'=8,'core'=2] {'core'}, dimensions={0}, use_global_device_ids=true | all-gather | bytes 589824 | tf_op jit(solution)/shard_map/all_gather | solution.py:237
  94.3 0.3 shard_map.186
  94.6 14.7 %all_to_all.34 = bf16[48,2,128]{2,1,0:T(2,128)(2,1)S(1)} all-to-all(bf16[48,2,128]{2,1,0:T(2,128)(2,1)S(1)} %bitcast.21), channel_id=1, replica_groups=mesh['ep'=48,'y'=8,'core'=2] {'ep'}, dimensions={0} | all-to-all | bytes 49152 | tf_op jit(solution)/shard_map/all_to_all | solution.py:338
  109.3 0.8 shard_map.187
  (25 shorter events, 0.1 us)
Async XLA Ops:
  0.0 1.0 copy-start.5
  1.0 0.8 copy-start.8
  1.9 0.7 copy-start.10
  2.6 14.7 %copy-start.14 = (bf16[2048,32]{0,1:T(8,128)(2,1)S(1)}, bf16[2048,32]{0,1:T(8,128)(2,1)}, u32[]{:S(2)}) copy-start(bf16[2048,32]{0,1:T(8,128)(2,1)} %param.25) | copy-start | bytes 393220
  3.5 20.8 %all-to-all-start = ((bf16[16,1,128]{2,1,0:T(2,128)(2,1)}), bf16[16,1,128]{2,1,0:T(2,128)(2,1)S(1)}, u32[]{:S(2)}, u32[]{:S(2)}) async-start(bf16[16,1,128]{2,1,0:T(2,128)(2,1)} %copy.21), calls=%async_computation | async-start | bytes 16384 | tf_op jit(solution)/shard_map/all_to_all | solution.py:272
  17.2 0.7 copy-start.16
  17.2 0.7 copy-start.18
  17.2 0.7 copy-start.15
  17.2 0.7 copy-start.17
  17.9 1.2 %copy-start.12 = (bf16[2048,256]{1,0:T(8,128)(2,1)S(1)}, bf16[2048,256]{1,0:T(8,128)(2,1)}, u32[]{:S(2)}) copy-start(bf16[2048,256]{1,0:T(8,128)(2,1)} %refs_2_.1) | copy-start | bytes 3145732
  19.1 1.2 %copy-start.13 = (bf16[2048,256]{1,0:T(8,128)(2,1)S(1)}, bf16[2048,256]{1,0:T(8,128)(2,1)}, u32[]{:S(2)}) copy-start(bf16[2048,256]{1,0:T(8,128)(2,1)} %refs_3_.1) | copy-start | bytes 3145732
  20.4 3.9 %copy-start = (bf16[1,2048,256]{2,1,0:T(8,128)(2,1)S(1)}, bf16[1,2048,256]{2,1,0:T(8,128)(2,1)}, u32[]{:S(2)}) copy-start(bf16[1,2048,256]{2,1,0:T(8,128)(2,1)} %keys_ref.1) | copy-start | bytes 3145732
  20.4 3.9 %copy-start.1 = (bf16[1,2048,256]{2,1,0:T(8,128)(2,1)S(1)}, bf16[1,2048,256]{2,1,0:T(8,128)(2,1)}, u32[]{:S(2)}) copy-start(bf16[1,2048,256]{2,1,0:T(8,128)(2,1)} %values_ref.1) | copy-start | bytes 3145732
  20.4 3.9 %copy-start.7 = (f32[1,32,2048]{2,1,0:T(8,128)S(1)}, f32[1,32,2048]{2,1,0:T(8,128)}, u32[]{:S(2)}) copy-start(f32[1,32,2048]{2,1,0:T(8,128)} %cum_ref.1) | copy-start | bytes 786436
  24.3 14.0 %copy-start.6 = (bf16[2048,128]{1,0:T(8,128)(2,1)S(1)}, bf16[2048,128]{1,0:T(8,128)(2,1)}, u32[]{:S(2)}) copy-start(bf16[2048,128]{1,0:T(8,128)(2,1)} %w_ref.4) | copy-start | bytes 1572868
  25.8 12.6 %copy-start.9 = (bf16[16,2048]{1,0:T(8,128)(2,1)S(1)}, bf16[16,2048]{1,0:T(8,128)(2,1)}, u32[]{:S(2)}) copy-start(bf16[16,2048]{1,0:T(8,128)(2,1)} %tokens_ref.3) | copy-start | bytes 196612
  62.3 15.9 %copy-start.3 = (bf16[1,2048,128]{2,1,0:T(8,128)(2,1)S(1)}, bf16[1,2048,128]{2,1,0:T(8,128)(2,1)}, u32[]{:S(2)}) copy-start(bf16[1,2048,128]{2,1,0:T(8,128)(2,1)} %w_up_ref.1) | copy-start | bytes 1572868
  62.3 15.8 %copy-start.2 = (bf16[1,2048,128]{2,1,0:T(8,128)(2,1)S(1)}, bf16[1,2048,128]{2,1,0:T(8,128)(2,1)}, u32[]{:S(2)}) copy-start(bf16[1,2048,128]{2,1,0:T(8,128)(2,1)} %w_gate_ref.1) | copy-start | bytes 1572868
  73.3 4.8 %copy-start.11 = (bf16[2048]{0:T(1024)(128)(2,1)S(1)}, bf16[2048]{0:T(1024)(128)(2,1)}, u32[]{:S(2)}) copy-start(bf16[2048]{0:T(1024)(128)(2,1)} %param.21) | copy-start | bytes 12292
  78.7 15.7 %copy-start.4 = (bf16[1,2048,128]{2,1,0:T(8,128)(2,1)S(1)}, bf16[1,2048,128]{2,1,0:T(8,128)(2,1)}, u32[]{:S(2)}) copy-start(bf16[1,2048,128]{2,1,0:T(8,128)(2,1)} %w_ref.5) | copy-start | bytes 1572868

commit v2 on v1

--- a/solution.py
+++ b/solution.py
@@ -15,21 +15,23 @@
 MASKED_SCORE = -1e30
 CORES = 2
 VMEM_LIMIT = 8 * 1024 * 1024
+HEAD_LIMIT = 67_043_328 - 3072 * 1024
 
 F32 = jnp.float32
 BF16 = jnp.bfloat16
 VM = pl.BlockSpec(memory_space=pltpu.VMEM)
+HB = pl.BlockSpec(memory_space=pltpu.HBM)
 SM = pl.BlockSpec(memory_space=pltpu.SMEM)
 
 
-def call(body, outs, operands, specs, scratch=(), flops=1_000_000, moved=1_000_000):
+def call(body, outs, operands, specs, scratch=(), flops=1_000_000, moved=1_000_000, limit=VMEM_LIMIT):
     return pl.pallas_call(
         body,
         out_shape=outs,
         in_specs=specs,
         out_specs=jax.tree.map(lambda _: VM, outs),
         scratch_shapes=list(scratch),
-        compiler_params=pltpu.CompilerParams(vmem_limit_bytes=VMEM_LIMIT),
+        compiler_params=pltpu.CompilerParams(vmem_limit_bytes=limit),
         cost_estimate=pl.CostEstimate(flops=flops, bytes_accessed=moved, transcendentals=0),
     )(*operands)
 
@@ -38,8 +40,65 @@
     return jax.ShapeDtypeStruct(shape, dtype)
 
 
-def query_kernel(tokens_ref, gain_ref, w_ref, normed_ref, query_ref):
+def held(shape, dtype):
+    return pltpu.VMEM(shape, dtype)
+
+
+def head_kernel(
+    place_ref,
+    length_hbm,
+    tokens_hbm,
+    gain_hbm,
+    w_query_hbm,
+    w_key_hbm,
+    w_value_hbm,
+    w_forget_hbm,
+    bias_hbm,
+    group_hbm,
+    expert_hbm,
+    weight_hbm,
+    query_ref,
+    key_ref,
+    value_ref,
+    gate_ref,
+    send_ref,
+    combine_ref,
+    used_ref,
+    residual_ref,
+    length_ref,
+    tokens_ref,
+    gain_ref,
+    w_query_ref,
+    w_key_ref,
+    w_value_ref,
+    w_forget_ref,
+    bias_ref,
+    group_ref,
+    expert_ref,
+    weight_ref,
+    sems,
+    *,
+    per_group,
+):
+    sources = (
+        tokens_hbm, gain_hbm, w_query_hbm, group_hbm, expert_hbm, weight_hbm, bias_hbm, w_forget_hbm,
+        w_key_hbm, w_value_hbm, length_hbm,
+    )
+    targets = (
+        tokens_ref, gain_ref, w_query_ref, group_ref, expert_ref, weight_ref, bias_ref, w_forget_ref,
+        w_key_ref, w_value_ref, length_ref,
+    )
+    loads = [
+        pltpu.make_async_copy(source, target, sems.at[i])
+        for i, (source, target) in enumerate(zip(sources, targets))
+    ]
+    for load in loads:
+        load.start()
+    for load in loads[:2]:
+        load.wait()
+    place = place_ref[0]
     values = tokens_ref[...].astype(F32)
+    rows = values.shape[0]
     mean = jnp.mean(values * values, axis=-1, keepdims=True)
     scaled = values * lax.rsqrt(mean + NORM_EPSILON)
     lanes = gain_ref.shape[1]
@@ -50,52 +109,11 @@
         ],
         axis=1,
     )
-    normed_ref[...] = normed
-    query_ref[...] = jnp.dot(normed, w_ref[...], preferred_element_type=F32).astype(BF16)
-
-
-def side_kernel(
-    place_ref,
-    normed_ref,
-    w_key_ref,
-    w_value_ref,
-    w_forget_ref,
-    bias_ref,
-    group_ref,
-    expert_ref,
-    weight_ref,
-    key_ref,
-    value_ref,
-    gate_ref,
-    send_ref,
-    combine_ref,
-    *,
-    per_group,
-):
-    place = place_ref[0]
-    normed = normed_ref[...]
-    rows = normed.shape[0]
-    own_row = lax.broadcasted_iota(jnp.int32, (rows, 1), 0) == place
-
-    def projected(w_ref):
-        full = jnp.dot(normed, w_ref[...], preferred_element_type=F32)
-        return jnp.sum(jnp.where(own_row, full, 0.0), axis=0, keepdims=True)
-
-    key_ref[...] = projected(w_key_ref).astype(BF16).astype(F32)
-    value_ref[...] = projected(w_value_ref).astype(BF16).astype(F32)
-    logits = lax.dot_general(
-        w_forget_ref[...], normed, (((1,), (1,)), ((), ())), preferred_element_type=F32
-    )
-    heads = logits.shape[0]
-    own_column = lax.broadcasted_iota(jnp.int32, (1, rows), 1) == place
-    logit = jnp.sum(jnp.where(own_column, logits, 0.0), axis=1, keepdims=True)
-    diagonal = lax.broadcasted_iota(jnp.int32, (heads, heads), 0) == lax.broadcasted_iota(
-        jnp.int32, (heads, heads), 1
-    )
-    bias = jnp.sum(jnp.where(diagonal, bias_ref[...], 0.0), axis=1, keepdims=True)
-    logit = logit + bias
-    log_gate = jnp.minimum(logit, 0.0) - jnp.log1p(jnp.exp(-jnp.abs(logit)))
-    gate_ref[...] = jnp.broadcast_to(log_gate, gate_ref.shape)
+    first = pl.multiple_of(place * lanes, lanes)
+    residual_ref[...] = tokens_ref[:, pl.ds(first, lanes)]
+    for load in loads[2:6]:
+        load.wait()
+    query_ref[...] = jnp.dot(normed, w_query_ref[...], preferred_element_type=F32).astype(BF16)
 
     picked = group_ref[...] * per_group + expert_ref[...]
     row_index = lax.broadcasted_iota(jnp.int32, (rows, rows), 0)
@@ -120,14 +138,43 @@
     send_ref[...] = send.astype(BF16)
     combine_ref[...] = combine
 
+    for load in loads[6:8]:
+        load.wait()
+    logits = lax.dot_general(
+        w_forget_ref[...], normed, (((1,), (1,)), ((), ())), preferred_element_type=F32
+    )
+    heads = QUERY_HEAD_COUNT
+    own_column = lax.broadcasted_iota(jnp.int32, (1, rows), 1) == place
+    logit = jnp.sum(jnp.where(own_column, logits, 0.0), axis=1, keepdims=True)
+    diagonal = lax.broadcasted_iota(jnp.int32, (heads, heads), 0) == lax.broadcasted_iota(
+        jnp.int32, (heads, heads), 1
+    )
+    bias = jnp.sum(jnp.where(diagonal, bias_ref[...], 0.0), axis=1, keepdims=True)
+    logit = logit + bias
+    log_gate = jnp.minimum(logit, 0.0) - jnp.log1p(jnp.exp(-jnp.abs(logit)))
+    gate_ref[...] = jnp.broadcast_to(log_gate, gate_ref.shape)
+
+    own_row = lax.broadcasted_iota(jnp.int32, (rows, 1), 0) == place
+
+    def projected(w_ref):
+        full = jnp.dot(normed, w_ref[...], preferred_element_type=F32)
+        return jnp.sum(jnp.where(own_row, full, 0.0), axis=0, keepdims=True)
+
+    loads[10].wait()
+    used_ref[...] = jnp.broadcast_to(length_ref[...], used_ref.shape)
+    loads[8].wait()
+    key_ref[...] = projected(w_key_ref).astype(BF16).astype(F32)
+    loads[9].wait()
+    value_ref[...] = projected(w_value_ref).astype(BF16).astype(F32)
+
 
 def attend_kernel(
-    length_ref, query_ref, key_new_ref, value_new_ref, gate_ref, keys_ref, values_ref, cum_ref, out_ref
+    used_ref, query_ref, key_ref, value_ref, gate_ref, keys_ref, values_ref, cum_ref, out_ref
 ):
     heads = QUERY_HEAD_COUNT
     pairs = heads // 2
     width = KV_HEADS * HEAD
-    used = length_ref[0]
+    used = used_ref[:1, :1]
 
     def index(shape, dim):
         return lax.broadcasted_iota(jnp.int32, shape, dim)
@@ -150,13 +197,13 @@
     scores = scores * (HEAD**-0.5) + latest + log_gate - cum
     usable = position < used
     scores = jnp.where(usable, scores, MASKED_SCORE)
-    own = jnp.sum(query_wide * key_new_ref[...], axis=1, keepdims=True) * (HEAD**-0.5)
+    own = jnp.sum(query_wide * key_ref[...], axis=1, keepdims=True) * (HEAD**-0.5)
     peak = jnp.maximum(jnp.max(scores, axis=1, keepdims=True), own)
     weights = jnp.where(usable, jnp.exp(scores - peak), 0.0)
     own_weight = jnp.exp(own - peak)
     denominator = jnp.sum(weights, axis=1, keepdims=True) + own_weight
     summed = jnp.dot(weights.astype(BF16), values_ref[0], preferred_element_type=F32)
-    summed = summed + own_weight.astype(BF16).astype(F32) * value_new_ref[...]
+    summed = summed + own_weight.astype(BF16).astype(F32) * value_ref[...]
     summed = jnp.where(in_block, summed, 0.0)
     summed = summed[:, : 2 * HEAD] + summed[:, 2 * HEAD :]
     summed = (summed[:, :HEAD] + summed[:, HEAD:]) / denominator
@@ -167,16 +214,14 @@
     out_ref[...] = jnp.broadcast_to(attended[None], out_ref.shape)
 
 
-def mix_kernel(place_ref, parts_ref, w_ref, tokens_ref, send_ref, mixed_ref, packed_ref, wide_ref):
+def mix_kernel(parts_ref, w_ref, residual_ref, send_ref, mixed_ref, packed_ref, wide_ref):
     rows, chunks, lanes = parts_ref.shape
     wide_ref[...] = parts_ref[...].reshape(rows * chunks, lanes).astype(F32)
     attended = jnp.concatenate(
         [wide_ref[pl.ds(i, rows, stride=chunks), :].astype(BF16) for i in range(chunks)], axis=1
     )
     projected = jnp.dot(attended, w_ref[...], preferred_element_type=F32)
-    first = pl.multiple_of(place_ref[0] * lanes, lanes)
-    residual = tokens_ref[:, pl.ds(first, lanes)].astype(F32)
-    mixed = (residual + projected).astype(BF16)
+    mixed = (residual_ref[...].astype(F32) + projected).astype(BF16)
     mixed_ref[...] = mixed
     packed_ref[...] = jnp.dot(send_ref[...], mixed, preferred_element_type=F32).astype(BF16)
 
@@ -262,57 +307,58 @@
         slots = experts * TOP
         place = (lax.axis_index("y") * CORES + lax.axis_index("core")).astype(jnp.int32)
         place = place.reshape(1)
-        normed, query = call(
-            query_kernel,
-            (shaped((rows, features), BF16), shaped((rows, part), BF16)),
-            (tokens, attn_gain.reshape(peers, part), w_query),
-            [VM] * 3,
-            flops=20_000_000,
+        def head(*refs):
+            head_kernel(*refs, per_group=experts // GROUPS)
+
+        kv = w_key.shape[1]
+        operands = (
+            cache_len.reshape(1, 1),
+            tokens,
+            attn_gain.reshape(peers, part),
+            w_query,
+            w_key,
+            w_value,
+            w_forget.T,
+            forget_bias.reshape(1, QUERY_HEAD_COUNT),
+            route_group.reshape(1, rows),
+            route_expert.T,
+            route_weight.T,
+        )
+        query, key_new, value_new, log_gate, send, combine, used, residual = call(
+            head,
+            (
+                held((rows, part), BF16),
+                held((1, kv), F32),
+                held((1, kv), F32),
+                held((QUERY_HEAD_COUNT, 128), F32),
+                held((slots, rows), BF16),
+                held((slots, rows), F32),
+                held((8, 128), jnp.int32),
+                held((rows, part), BF16),
+            ),
+            (place, *operands),
+            [SM] + [HB] * len(operands),
+            scratch=[pltpu.VMEM(one.shape, one.dtype) for one in operands]
+            + [pltpu.SemaphoreType.DMA((len(operands),))],
+            flops=50_000_000,
+            limit=HEAD_LIMIT,
         )
         own_query = lax.all_to_all(
             query.reshape(peers, 1, part), tp, split_axis=0, concat_axis=0, tiled=True
         ).reshape(peers, part)
-
-        def side(*refs):
-            side_kernel(*refs, per_group=experts // GROUPS)
-
-        kv = w_key.shape[1]
-        key_new, value_new, log_gate, send, combine = call(
-            side,
-            (
-                shaped((1, kv), F32),
-                shaped((1, kv), F32),
-                shaped((QUERY_HEAD_COUNT, 128), F32),
-                shaped((slots, rows), BF16),
-                shaped((slots, rows), F32),
-            ),
-            (
-                place,
-                normed,
-                w_key,
-                w_value,
-                w_forget.T,
-                forget_bias.reshape(1, QUERY_HEAD_COUNT),
-                route_group.reshape(1, rows),
-                route_expert.T,
-                route_weight.T,
-            ),
-            [SM] + [VM] * 8,
-            flops=2_000_000_000,
-        )
         copies = call(
             attend_kernel,
             shaped((peers, peers, part), BF16),
-            (cache_len, own_query, key_new, value_new, log_gate, cache_keys, cache_values, cache_logcum),
-            [SM] + [VM] * 7,
+            (used, own_query, key_new, value_new, log_gate, cache_keys, cache_values, cache_logcum),
+            [VM] * 8,
             flops=200_000_000,
         )
         attended = lax.all_to_all(copies, tp, 0, 0, tiled=True)
         mixed, packed = call(
             mix_kernel,
             (shaped((rows, part), BF16), shaped((slots, part), BF16)),
-            (place, attended, w_out, tokens, send),
-            [SM] + [VM] * 4,
+            (attended, w_out, residual, send),
+            [VM] * 4,
             scratch=[pltpu.VMEM((rows * peers, part), F32)],
             flops=20_000_000,
         )

time: 111 us -> 108 us (0.973)
  blocking collectives: 82.4 us -> 101 us
  starting transfers between devices: 13.7 us -> 0 us
  local copies, waits for them, and re-layouts: 6.38 us -> 0.08 us
  waiting for transfers between devices: 2.56 us -> 0 us
  Pallas kernels: 4.13 us -> 5.98 us
    all_to_all x0 -> x1, blocking collectives: none -> 20 us  [on_device(): lax.all_to_all(query.reshape(peers, 1, part), tp, split_axis=0, concat_ax...]
    all_to_all x1 -> x0, starting transfers between devices: 13.7 us -> none  [on_device(): lax.all_to_all(query.reshape(peers, 1, part), tp, split_axis=0, concat_ax...]
    unnamed x39 -> x17, local copies, waits for them, and re-layouts: 5.74 us -> 0.04 us
    all_to_all x1 -> x0, waiting for transfers between devices: 2.56 us -> none  [on_device(): lax.all_to_all(query.reshape(peers, 1, part), tp, split_axis=0, concat_ax...]
    pallas_call x7 -> x6, Pallas kernels: 4.13 us -> 5.98 us  [call(): pl.pallas_call(body, out_shape=outs, in_specs=specs, out_specs=jax.tree.m...]
    all_to_all x1, blocking collectives: 12.6 us -> 10.9 us  [on_device(): attended = lax.all_to_all(copies, tp, 0, 0, tiled=True)]
  transfers between devices with their start and end apart: 1 -> 0, of which waited for: 1 -> 0; matrix products, arithmetic and copies ran while one was open for 0% -> 0% of each run, Pallas kernels for 0% -> 0%
where the time goes in v2:
time: 108 us
  blocking collectives  101 us (94%)
  Pallas kernels  5.98 us (6%)
    all_to_all x1, blocking collectives, on_device(): lax.all_to_all(packed.reshape(experts, TOP, part), 'ep', 0, 0, tiled=True)  24.3 us
    all_to_all x2, blocking collectives, to_all(): exchanged = lax.all_to_all(copies, 'y', 0, 0, tiled=True)  23.7 us
    all_to_all x1, blocking collectives, on_device(): lax.all_to_all(query.reshape(peers, 1, part), tp, split_axis=0, concat_ax...  20 us
    all_to_all x1, blocking collectives, on_device(): lax.all_to_all(result.reshape(experts, TOP, part), 'ep', 0, 0, tiled=True)  14.7 us
    all_to_all x1, blocking collectives, on_device(): attended = lax.all_to_all(copies, tp, 0, 0, tiled=True)  10.9 us
    all_gather x2, blocking collectives, to_all(): return lax.all_gather(exchanged, 'core', axis=0, tiled=False)  7.81 us
    pallas_call x6, Pallas kernels, call(): pl.pallas_call(body, out_shape=outs, in_specs=specs, out_specs=jax.tree.m...  5.98 us

profile of v2, /device:TPU:1, one launch (start us, length us, event | category | flops | bytes accessed | tf_op | source)
XLA Modules:
  0.0 108.1 jit_solution(4327711166491302936)
XLA Ops:
  0.7 0.0 copy-start
  0.7 0.0 copy-start.1
  0.7 0.0 copy-start.6
  0.7 2.7 %shard_map.181 = (bf16[16,128]{1,0:T(8,128)(2,1)S(1)}, f32[1,256]{1,0:T(1,128)S(1)}, f32[1,256]{1,0:T(1,128)S(1)}, f32[32,128]{1,0:T(8,128)S(1)}, bf16[96,16]{1,...) custom-call(s32[1]{0:T(128)} %bitcast.refs_0_, ...), custom_call_target="tpu_custom_call" | custom-call | flops 50000000 | bytes 1000000 | tf_op jit(solution)/shard_map/pallas_call | solution.py:28
  3.4 20.0 %all_to_all.30 = bf16[16,1,128]{2,1,0:T(2,128)(2,1)S(1)} all-to-all(bf16[16,1,128]{2,1,0:T(2,128)(2,1)S(1)} %copy.21), channel_id=1, replica_groups=mesh['ep'=48,'y'=8,'core'=2] {'y','core'}, dimensions={0} | all-to-all | bytes 8192 | tf_op jit(solution)/shard_map/all_to_all | solution.py:346
  23.3 0.0 copy-done
  23.3 0.0 copy-done.1
  23.3 0.0 copy-done.6
  23.4 0.0 copy-start.5
  23.4 1.4 %shard_map.182 = bf16[16,16,128]{2,1,0:T(8,128)(2,1)S(1)} custom-call(s32[8,128]{1,0:T(8,128)S(1)} %get-tuple-element.15.used_ref, bf16[16,128]{1,0:T(8,128)(2,1)S(1)} %bitcast.25, f32[1,256]{1,0:T(1,128)S(1)} %get-tuple-element.17.key_ref, f32[1,256]{1,0:T(1,128)S(1)} %get-tuple-element.18.value_ref, f32[32,128]{1,0:T(8,128)S(1)} %get-tuple-element.19.gate_ref, ...), custom_call_target="tpu_custom_call" | custom-call | flops 200000000 | bytes 1000000 | tf_op jit(solution)/shard_map/pallas_call | solution.py:28
  24.8 10.9 %all_to_all.31.parts_ref = bf16[16,16,128]{2,1,0:T(8,128)(2,1)S(1)} all-to-all(bf16[16,16,128]{2,1,0:T(8,128)(2,1)S(1)} %shard_map.182), channel_id=1, replica_groups=mesh['ep'=48,'y'=8,'core'=2] {'y','core'}, dimensions={0} | all-to-all | bytes 131072 | tf_op jit(solution)/shard_map/all_to_all | solution.py:356
  35.7 0.0 copy-done.5
  35.7 0.3 shard_map.183
  36.0 24.3 %all_to_all.32 = bf16[48,2,128]{2,1,0:T(2,128)(2,1)S(1)} all-to-all(bf16[48,2,128]{2,1,0:T(2,128)(2,1)S(1)} %bitcast.24), channel_id=1, replica_groups=mesh['ep'=48,'y'=8,'core'=2] {'ep'}, dimensions={0} | all-to-all | bytes 49152 | tf_op jit(solution)/shard_map/all_to_all | solution.py:365
  60.3 0.0 copy-start.3
  60.3 0.0 copy-start.2
  60.3 11.1 %all_to_all.33 = bf16[8,96,128]{2,1,0:T(8,128)(2,1)S(1)} all-to-all(bf16[8,96,128]{2,1,0:T(8,128)(2,1)S(1)} %broadcast_in_dim.8), channel_id=1, replica_groups=mesh['ep'=48,'y'=8,'core'=2] {'y'}, dimensions={0} | all-to-all | bytes 393216 | tf_op jit(solution)/shard_map/all_to_all | solution.py:281
  71.4 0.0 copy-start.7
  71.4 4.7 %all-gather = bf16[16,96,128]{2,1,0:T(8,128)(2,1)S(1)} all-gather(bf16[8,96,128]{2,1,0:T(8,128)(2,1)S(1)} %all_to_all.33), channel_id=2, replica_groups=mesh['ep'=48,'y'=8,'core'=2] {'core'}, dimensions={0}, use_global_device_ids=true | all-gather | bytes 589824 | tf_op jit(solution)/shard_map/all_gather | solution.py:282
  76.1 0.0 copy-done.3
  76.1 0.0 copy-done.2
  76.1 0.0 copy-done.7
  76.1 0.5 shard_map.184
  76.7 0.0 copy-start.4
  76.7 12.6 %all_to_all.34 = bf16[8,96,128]{2,1,0:T(8,128)(2,1)S(1)} all-to-all(bf16[8,96,128]{2,1,0:T(8,128)(2,1)S(1)} %shard_map.184), channel_id=1, replica_groups=mesh['ep'=48,'y'=8,'core'=2] {'y'}, dimensions={0} | all-to-all | bytes 393216 | tf_op jit(solution)/shard_map/all_to_all | solution.py:281
  89.2 3.1 %all-gather.1 = bf16[16,96,128]{2,1,0:T(8,128)(2,1)S(1)} all-gather(bf16[8,96,128]{2,1,0:T(8,128)(2,1)S(1)} %all_to_all.34), channel_id=3, replica_groups=mesh['ep'=48,'y'=8,'core'=2] {'core'}, dimensions={0}, use_global_device_ids=true | all-gather | bytes 589824 | tf_op jit(solution)/shard_map/all_gather | solution.py:282
  92.3 0.0 copy-done.4
  92.3 0.3 shard_map.185
  92.6 14.7 %all_to_all.35 = bf16[48,2,128]{2,1,0:T(2,128)(2,1)S(1)} all-to-all(bf16[48,2,128]{2,1,0:T(2,128)(2,1)S(1)} %bitcast.23), channel_id=1, replica_groups=mesh['ep'=48,'y'=8,'core'=2] {'ep'}, dimensions={0} | all-to-all | bytes 49152 | tf_op jit(solution)/shard_map/all_to_all | solution.py:384
  107.3 0.8 shard_map.186
  (3 shorter events, 0.0 us)
Async XLA Ops:
  0.7 22.7 %copy-start = (bf16[1,2048,256]{2,1,0:T(8,128)(2,1)S(1)}, bf16[1,2048,256]{2,1,0:T(8,128)(2,1)}, u32[]{:S(2)}) copy-start(bf16[1,2048,256]{2,1,0:T(8,128)(2,1)} %keys_ref.1) | copy-start | bytes 3145732
  0.7 22.7 %copy-start.1 = (bf16[1,2048,256]{2,1,0:T(8,128)(2,1)S(1)}, bf16[1,2048,256]{2,1,0:T(8,128)(2,1)}, u32[]{:S(2)}) copy-start(bf16[1,2048,256]{2,1,0:T(8,128)(2,1)} %values_ref.1) | copy-start | bytes 3145732
  0.7 22.7 %copy-start.6 = (f32[1,32,2048]{2,1,0:T(8,128)S(1)}, f32[1,32,2048]{2,1,0:T(8,128)}, u32[]{:S(2)}) copy-start(f32[1,32,2048]{2,1,0:T(8,128)} %cum_ref.1) | copy-start | bytes 786436
  23.4 12.3 %copy-start.5 = (bf16[2048,128]{1,0:T(8,128)(2,1)S(1)}, bf16[2048,128]{1,0:T(8,128)(2,1)}, u32[]{:S(2)}) copy-start(bf16[2048,128]{1,0:T(8,128)(2,1)} %w_ref.2) | copy-start | bytes 1572868
  60.3 15.9 %copy-start.3 = (bf16[1,2048,128]{2,1,0:T(8,128)(2,1)S(1)}, bf16[1,2048,128]{2,1,0:T(8,128)(2,1)}, u32[]{:S(2)}) copy-start(bf16[1,2048,128]{2,1,0:T(8,128)(2,1)} %w_up_ref.1) | copy-start | bytes 1572868
  60.3 15.8 %copy-start.2 = (bf16[1,2048,128]{2,1,0:T(8,128)(2,1)S(1)}, bf16[1,2048,128]{2,1,0:T(8,128)(2,1)}, u32[]{:S(2)}) copy-start(bf16[1,2048,128]{2,1,0:T(8,128)(2,1)} %w_gate_ref.1) | copy-start | bytes 1572868
  71.4 4.7 %copy-start.7 = (bf16[2048]{0:T(1024)(128)(2,1)S(1)}, bf16[2048]{0:T(1024)(128)(2,1)}, u32[]{:S(2)}) copy-start(bf16[2048]{0:T(1024)(128)(2,1)} %param.21) | copy-start | bytes 12292
  76.7 15.7 %copy-start.4 = (bf16[1,2048,128]{2,1,0:T(8,128)(2,1)S(1)}, bf16[1,2048,128]{2,1,0:T(8,128)(2,1)}, u32[]{:S(2)}) copy-start(bf16[1,2048,128]{2,1,0:T(8,128)(2,1)} %w_ref.3) | copy-start | bytes 1572868

commit v3 on v2

--- a/solution.py
+++ b/solution.py
@@ -15,7 +15,7 @@
 MASKED_SCORE = -1e30
 CORES = 2
 VMEM_LIMIT = 8 * 1024 * 1024
-HEAD_LIMIT = 67_043_328 - 3072 * 1024
+HEAD_LIMIT = 67_043_328 - 512 * 1024
 
 F32 = jnp.float32
 BF16 = jnp.bfloat16
@@ -50,17 +50,13 @@
     tokens_hbm,
     gain_hbm,
     w_query_hbm,
-    w_key_hbm,
-    w_value_hbm,
-    w_forget_hbm,
     bias_hbm,
     group_hbm,
     expert_hbm,
     weight_hbm,
     query_ref,
-    key_ref,
-    value_ref,
-    gate_ref,
+    normed_ref,
+    bias_out_ref,
     send_ref,
     combine_ref,
     used_ref,
@@ -69,9 +65,6 @@
     tokens_ref,
     gain_ref,
     w_query_ref,
-    w_key_ref,
-    w_value_ref,
-    w_forget_ref,
     bias_ref,
     group_ref,
     expert_ref,
@@ -81,12 +74,10 @@
     per_group,
 ):
     sources = (
-        tokens_hbm, gain_hbm, w_query_hbm, group_hbm, expert_hbm, weight_hbm, bias_hbm, w_forget_hbm,
-        w_key_hbm, w_value_hbm, length_hbm,
+        tokens_hbm, gain_hbm, w_query_hbm, group_hbm, expert_hbm, weight_hbm, bias_hbm, length_hbm
     )
     targets = (
-        tokens_ref, gain_ref, w_query_ref, group_ref, expert_ref, weight_ref, bias_ref, w_forget_ref,
-        w_key_ref, w_value_ref, length_ref,
+        tokens_ref, gain_ref, w_query_ref, group_ref, expert_ref, weight_ref, bias_ref, length_ref
     )
     loads = [
         pltpu.make_async_copy(source, target, sems.at[i])
@@ -96,7 +87,6 @@
         load.start()
     for load in loads[:2]:
         load.wait()
-    place = place_ref[0]
     values = tokens_ref[...].astype(F32)
     rows = values.shape[0]
     mean = jnp.mean(values * values, axis=-1, keepdims=True)
@@ -109,9 +99,10 @@
         ],
         axis=1,
     )
-    first = pl.multiple_of(place * lanes, lanes)
+    normed_ref[...] = normed
+    first = pl.multiple_of(place_ref[0] * lanes, lanes)
     residual_ref[...] = tokens_ref[:, pl.ds(first, lanes)]
-    for load in loads[2:6]:
+    for load in loads[2:]:
         load.wait()
     query_ref[...] = jnp.dot(normed, w_query_ref[...], preferred_element_type=F32).astype(BF16)
 
@@ -138,39 +129,51 @@
     send_ref[...] = send.astype(BF16)
     combine_ref[...] = combine
 
-    for load in loads[6:8]:
-        load.wait()
+    heads = QUERY_HEAD_COUNT
+    diagonal = lax.broadcasted_iota(jnp.int32, (heads, heads), 0) == lax.broadcasted_iota(
+        jnp.int32, (heads, heads), 1
+    )
+    bias = jnp.sum(jnp.where(diagonal, bias_ref[...], 0.0), axis=1, keepdims=True)
+    bias_out_ref[...] = jnp.broadcast_to(bias, bias_out_ref.shape)
+    used_ref[...] = jnp.broadcast_to(length_ref[...], used_ref.shape)
+
+
+def pass_kernel(query_ref, out_ref):
+    out_ref[...] = query_ref[...]
+
+
+def attend_kernel(
+    place_ref,
+    used_ref,
+    query_ref,
+    normed_ref,
+    w_key_ref,
+    w_value_ref,
+    w_forget_ref,
+    bias_ref,
+    keys_ref,
+    values_ref,
+    cum_ref,
+    out_ref,
+):
+    place = place_ref[0]
+    normed = normed_ref[...]
+    rows = normed.shape[0]
+    own_row = lax.broadcasted_iota(jnp.int32, (rows, 1), 0) == place
+    own_column = lax.broadcasted_iota(jnp.int32, (1, rows), 1) == place
+
+    def projected(w_ref):
+        full = jnp.dot(normed, w_ref[...], preferred_element_type=F32)
+        one = jnp.sum(jnp.where(own_row, full, 0.0), axis=0, keepdims=True)
+        return one.astype(BF16).astype(F32)
+
+    key_new = projected(w_key_ref)
+    value_new = projected(w_value_ref)
     logits = lax.dot_general(
         w_forget_ref[...], normed, (((1,), (1,)), ((), ())), preferred_element_type=F32
     )
-    heads = QUERY_HEAD_COUNT
-    own_column = lax.broadcasted_iota(jnp.int32, (1, rows), 1) == place
-    logit = jnp.sum(jnp.where(own_column, logits, 0.0), axis=1, keepdims=True)
-    diagonal = lax.broadcasted_iota(jnp.int32, (heads, heads), 0) == lax.broadcasted_iota(
-        jnp.int32, (heads, heads), 1
-    )
-    bias = jnp.sum(jnp.where(diagonal, bias_ref[...], 0.0), axis=1, keepdims=True)
-    logit = logit + bias
+    logit = jnp.sum(jnp.where(own_column, logits, 0.0), axis=1, keepdims=True) + bias_ref[:, :1]
     log_gate = jnp.minimum(logit, 0.0) - jnp.log1p(jnp.exp(-jnp.abs(logit)))
-    gate_ref[...] = jnp.broadcast_to(log_gate, gate_ref.shape)
-
-    own_row = lax.broadcasted_iota(jnp.int32, (rows, 1), 0) == place
-
-    def projected(w_ref):
-        full = jnp.dot(normed, w_ref[...], preferred_element_type=F32)
-        return jnp.sum(jnp.where(own_row, full, 0.0), axis=0, keepdims=True)
-
-    loads[10].wait()
-    used_ref[...] = jnp.broadcast_to(length_ref[...], used_ref.shape)
-    loads[8].wait()
-    key_ref[...] = projected(w_key_ref).astype(BF16).astype(F32)
-    loads[9].wait()
-    value_ref[...] = projected(w_value_ref).astype(BF16).astype(F32)
-
-
-def attend_kernel(
-    used_ref, query_ref, key_ref, value_ref, gate_ref, keys_ref, values_ref, cum_ref, out_ref
-):
     heads = QUERY_HEAD_COUNT
     pairs = heads // 2
     width = KV_HEADS * HEAD
@@ -191,19 +194,18 @@
         query_all, keys_ref[0], (((1,), (1,)), ((), ())), preferred_element_type=F32
     )
     cum = cum_ref[0]
-    log_gate = gate_ref[:, :1]
     position = lax.broadcasted_iota(jnp.int32, scores.shape, 1)
     latest = jnp.sum(jnp.where(position == used - 1, cum, 0.0), axis=1, keepdims=True)
     scores = scores * (HEAD**-0.5) + latest + log_gate - cum
     usable = position < used
     scores = jnp.where(usable, scores, MASKED_SCORE)
-    own = jnp.sum(query_wide * key_ref[...], axis=1, keepdims=True) * (HEAD**-0.5)
+    own = jnp.sum(query_wide * key_new, axis=1, keepdims=True) * (HEAD**-0.5)
     peak = jnp.maximum(jnp.max(scores, axis=1, keepdims=True), own)
     weights = jnp.where(usable, jnp.exp(scores - peak), 0.0)
     own_weight = jnp.exp(own - peak)
     denominator = jnp.sum(weights, axis=1, keepdims=True) + own_weight
     summed = jnp.dot(weights.astype(BF16), values_ref[0], preferred_element_type=F32)
-    summed = summed + own_weight.astype(BF16).astype(F32) * value_ref[...]
+    summed = summed + own_weight.astype(BF16).astype(F32) * value_new
     summed = jnp.where(in_block, summed, 0.0)
     summed = summed[:, : 2 * HEAD] + summed[:, 2 * HEAD :]
     summed = (summed[:, :HEAD] + summed[:, HEAD:]) / denominator
@@ -310,26 +312,21 @@
         def head(*refs):
             head_kernel(*refs, per_group=experts // GROUPS)
 
-        kv = w_key.shape[1]
         operands = (
             cache_len.reshape(1, 1),
             tokens,
             attn_gain.reshape(peers, part),
             w_query,
-            w_key,
-            w_value,
-            w_forget.T,
             forget_bias.reshape(1, QUERY_HEAD_COUNT),
             route_group.reshape(1, rows),
             route_expert.T,
             route_weight.T,
         )
-        query, key_new, value_new, log_gate, send, combine, used, residual = call(
+        query, normed, bias, send, combine, used, residual = call(
             head,
             (
                 held((rows, part), BF16),
-                held((1, kv), F32),
-                held((1, kv), F32),
+                held((rows, features), BF16),
                 held((QUERY_HEAD_COUNT, 128), F32),
                 held((slots, rows), BF16),
                 held((slots, rows), F32),
@@ -340,8 +337,15 @@
             [SM] + [HB] * len(operands),
             scratch=[pltpu.VMEM(one.shape, one.dtype) for one in operands]
             + [pltpu.SemaphoreType.DMA((len(operands),))],
-            flops=50_000_000,
+            flops=10_000_000,
             limit=HEAD_LIMIT,
+        )
+        query = call(
+            pass_kernel,
+            held((rows, part), BF16),
+            (query,),
+            [VM],
+            flops=20_000_000_000,
         )
         own_query = lax.all_to_all(
             query.reshape(peers, 1, part), tp, split_axis=0, concat_axis=0, tiled=True
@@ -349,8 +353,20 @@
         copies = call(
             attend_kernel,
             shaped((peers, peers, part), BF16),
-            (used, own_query, key_new, value_new, log_gate, cache_keys, cache_values, cache_logcum),
-            [VM] * 8,
+            (
+                place,
+                used,
+                own_query,
+                normed,
+                w_key,
+                w_value,
+                w_forget.T,
+                bias,
+                cache_keys,
+                cache_values,
+                cache_logcum,
+            ),
+            [SM] + [VM] * 10,
             flops=200_000_000,
         )
         attended = lax.all_to_all(copies, tp, 0, 0, tiled=True)

time: 108 us -> 108 us (level)
  Pallas kernels: 5.98 us -> 4.9 us
    pallas_call x6 -> x7, Pallas kernels: 5.98 us -> 4.9 us  [call(): pl.pallas_call(body, out_shape=outs, in_specs=specs, out_specs=jax.tree.m...]
where the time goes in v3:
time: 108 us; the launch traced here: 107 us
  blocking collectives  102 us (94%)
  Pallas kernels  4.9 us (5%)
    all_to_all x1, blocking collectives, on_device(): lax.all_to_all(packed.reshape(experts, TOP, part), 'ep', 0, 0, tiled=True)  24.3 us
    all_to_all x2, blocking collectives, to_all(): exchanged = lax.all_to_all(copies, 'y', 0, 0, tiled=True)  23.6 us
    all_to_all x1, blocking collectives, on_device(): lax.all_to_all(query.reshape(peers, 1, part), tp, split_axis=0, concat_ax...  20.2 us
    all_to_all x1, blocking collectives, on_device(): lax.all_to_all(result.reshape(experts, TOP, part), 'ep', 0, 0, tiled=True)  14.7 us
    all_to_all x1, blocking collectives, on_device(): attended = lax.all_to_all(copies, tp, 0, 0, tiled=True)  10.9 us
    all_gather x2, blocking collectives, to_all(): return lax.all_gather(exchanged, 'core', axis=0, tiled=False)  7.83 us
    pallas_call x7, Pallas kernels, call(): pl.pallas_call(body, out_shape=outs, in_specs=specs, out_specs=jax.tree.m...  4.9 us

profile of v3, /device:TPU:1, one launch (start us, length us, event | category | flops | bytes accessed | tf_op | source)
XLA Modules:
  0.0 107.4 jit_solution(13532099952190276418)
XLA Ops:
  0.7 1.4 %shard_map.181 = (bf16[16,128]{1,0:T(8,128)(2,1)S(1)}, bf16[16,2048]{1,0:T(8,128)(2,1)S(1)}, f32[32,128]{1,0:T(8,128)S(1)}, bf16[96,16]{1,0:T(8,128)(2,1)S(1)}, ...) custom-call(s32[1]{0:T(128)} %bitcast.refs_0_.place_ref, s32[1,1]{1,0:T(1,128)} %bitcast.19.refs_1_, ...), custom_call_target="tpu_custom_call" | custom-call | flops 10000000 | bytes 1000000 | tf_op jit(solution)/shard_map/pallas_call | solution.py:28
  2.0 0.0 copy-start
  2.0 0.0 copy-start.1
  2.1 0.0 copy-start.2
  2.1 0.0 copy-start.3
  2.1 0.0 copy-start.8
  2.1 0.0 copy-start.9
  2.1 20.2 %all_to_all.30 = bf16[16,1,128]{2,1,0:T(2,128)(2,1)S(1)} all-to-all(bf16[16,1,128]{2,1,0:T(2,128)(2,1)S(1)} %copy.21), channel_id=1, replica_groups=mesh['ep'=48,'y'=8,'core'=2] {'y','core'}, dimensions={0} | all-to-all | bytes 8192 | tf_op jit(solution)/shard_map/all_to_all | solution.py:350
  22.4 0.0 copy-done
  22.4 0.0 copy-done.1
  22.4 0.0 copy-done.2
  22.4 0.0 copy-done.3
  22.4 0.0 copy-done.8
  22.4 0.0 copy-done.9
  22.4 0.0 copy-start.7
  22.4 1.6 %shard_map.183 = bf16[16,16,128]{2,1,0:T(8,128)(2,1)S(1)} custom-call(s32[1]{0:T(128)} %bitcast.refs_0_.place_ref, s32[8,128]{1,0:T(8,128)S(1)} %get-tuple-element.14.used_ref, bf16[16,128]{1,0:T(8,128)(2,1)S(1)} %bitcast.26, bf16[16,2048]{1,0:T(8,128)(2,1)S(1)} %get-tuple-element.16.normed_ref, bf16[2048,256]{1,0:T(8,128)(2,1)S(1)} %copy-done, ...), custom_call_target="tpu_custom_call" | custom-call | flops 200000000 | bytes 1000000 | tf_op jit(solution)/shard_map/pallas_call | solution.py:28
  24.1 10.9 %all_to_all.31.parts_ref = bf16[16,16,128]{2,1,0:T(8,128)(2,1)S(1)} all-to-all(bf16[16,16,128]{2,1,0:T(8,128)(2,1)S(1)} %shard_map.183), channel_id=1, replica_groups=mesh['ep'=48,'y'=8,'core'=2] {'y','core'}, dimensions={0} | all-to-all | bytes 131072 | tf_op jit(solution)/shard_map/all_to_all | solution.py:372
  35.0 0.0 copy-done.7
  35.0 0.3 shard_map.184
  35.3 24.3 %all_to_all.32 = bf16[48,2,128]{2,1,0:T(2,128)(2,1)S(1)} all-to-all(bf16[48,2,128]{2,1,0:T(2,128)(2,1)S(1)} %bitcast.25), channel_id=1, replica_groups=mesh['ep'=48,'y'=8,'core'=2] {'ep'}, dimensions={0} | all-to-all | bytes 49152 | tf_op jit(solution)/shard_map/all_to_all | solution.py:381
  59.6 0.0 copy-start.4
  59.6 11.1 %all_to_all.33 = bf16[8,96,128]{2,1,0:T(8,128)(2,1)S(1)} all-to-all(bf16[8,96,128]{2,1,0:T(8,128)(2,1)S(1)} %broadcast_in_dim.8), channel_id=1, replica_groups=mesh['ep'=48,'y'=8,'core'=2] {'y'}, dimensions={0} | all-to-all | bytes 393216 | tf_op jit(solution)/shard_map/all_to_all | solution.py:283
  70.7 4.7 %all-gather = bf16[16,96,128]{2,1,0:T(8,128)(2,1)S(1)} all-gather(bf16[8,96,128]{2,1,0:T(8,128)(2,1)S(1)} %all_to_all.33), channel_id=2, replica_groups=mesh['ep'=48,'y'=8,'core'=2] {'core'}, dimensions={0}, use_global_device_ids=true | all-gather | bytes 589824 | tf_op jit(solution)/shard_map/all_gather | solution.py:284
  75.4 0.0 copy-done.5
  75.4 0.0 copy-done.4
  75.4 0.5 shard_map.185
  75.9 0.0 copy-start.6
  75.9 12.5 %all_to_all.34 = bf16[8,96,128]{2,1,0:T(8,128)(2,1)S(1)} all-to-all(bf16[8,96,128]{2,1,0:T(8,128)(2,1)S(1)} %shard_map.185), channel_id=1, replica_groups=mesh['ep'=48,'y'=8,'core'=2] {'y'}, dimensions={0} | all-to-all | bytes 393216 | tf_op jit(solution)/shard_map/all_to_all | solution.py:283
  88.5 3.1 %all-gather.1 = bf16[16,96,128]{2,1,0:T(8,128)(2,1)S(1)} all-gather(bf16[8,96,128]{2,1,0:T(8,128)(2,1)S(1)} %all_to_all.34), channel_id=3, replica_groups=mesh['ep'=48,'y'=8,'core'=2] {'core'}, dimensions={0}, use_global_device_ids=true | all-gather | bytes 589824 | tf_op jit(solution)/shard_map/all_gather | solution.py:284
  91.6 0.3 shard_map.186
  91.9 14.7 %all_to_all.35 = bf16[48,2,128]{2,1,0:T(2,128)(2,1)S(1)} all-to-all(bf16[48,2,128]{2,1,0:T(2,128)(2,1)S(1)} %bitcast.24), channel_id=1, replica_groups=mesh['ep'=48,'y'=8,'core'=2] {'ep'}, dimensions={0} | all-to-all | bytes 49152 | tf_op jit(solution)/shard_map/all_to_all | solution.py:400
  106.6 0.8 shard_map.187
  (8 shorter events, 0.0 us)
Async XLA Ops:
  2.0 20.3 %copy-start = (bf16[2048,256]{1,0:T(8,128)(2,1)S(1)}, bf16[2048,256]{1,0:T(8,128)(2,1)}, u32[]{:S(2)}) copy-start(bf16[2048,256]{1,0:T(8,128)(2,1)} %w_key_ref.1) | copy-start | bytes 3145732
  2.0 20.3 %copy-start.1 = (bf16[2048,256]{1,0:T(8,128)(2,1)S(1)}, bf16[2048,256]{1,0:T(8,128)(2,1)}, u32[]{:S(2)}) copy-start(bf16[2048,256]{1,0:T(8,128)(2,1)} %w_value_ref.1) | copy-start | bytes 3145732
  2.1 20.3 %copy-start.2 = (bf16[1,2048,256]{2,1,0:T(8,128)(2,1)S(1)}, bf16[1,2048,256]{2,1,0:T(8,128)(2,1)}, u32[]{:S(2)}) copy-start(bf16[1,2048,256]{2,1,0:T(8,128)(2,1)} %keys_ref.1) | copy-start | bytes 3145732
  2.1 20.3 %copy-start.3 = (bf16[1,2048,256]{2,1,0:T(8,128)(2,1)S(1)}, bf16[1,2048,256]{2,1,0:T(8,128)(2,1)}, u32[]{:S(2)}) copy-start(bf16[1,2048,256]{2,1,0:T(8,128)(2,1)} %values_ref.1) | copy-start | bytes 3145732
  2.1 20.3 %copy-start.8 = (f32[1,32,2048]{2,1,0:T(8,128)S(1)}, f32[1,32,2048]{2,1,0:T(8,128)}, u32[]{:S(2)}) copy-start(f32[1,32,2048]{2,1,0:T(8,128)} %cum_ref.1) | copy-start | bytes 786436
  2.1 20.3 %copy-start.9 = (bf16[2048,32]{0,1:T(8,128)(2,1)S(1)}, bf16[2048,32]{0,1:T(8,128)(2,1)}, u32[]{:S(2)}) copy-start(bf16[2048,32]{0,1:T(8,128)(2,1)} %param.25) | copy-start | bytes 393220
  22.4 12.6 %copy-start.7 = (bf16[2048,128]{1,0:T(8,128)(2,1)S(1)}, bf16[2048,128]{1,0:T(8,128)(2,1)}, u32[]{:S(2)}) copy-start(bf16[2048,128]{1,0:T(8,128)(2,1)} %w_ref.2) | copy-start | bytes 1572868
  59.5 15.9 %copy-start.5 = (bf16[1,2048,128]{2,1,0:T(8,128)(2,1)S(1)}, bf16[1,2048,128]{2,1,0:T(8,128)(2,1)}, u32[]{:S(2)}) copy-start(bf16[1,2048,128]{2,1,0:T(8,128)(2,1)} %w_up_ref.1) | copy-start | bytes 1572868
  59.6 15.8 %copy-start.4 = (bf16[1,2048,128]{2,1,0:T(8,128)(2,1)S(1)}, bf16[1,2048,128]{2,1,0:T(8,128)(2,1)}, u32[]{:S(2)}) copy-start(bf16[1,2048,128]{2,1,0:T(8,128)(2,1)} %w_gate_ref.1) | copy-start | bytes 1572868
  70.7 4.7 %copy-start.10 = (bf16[2048]{0:T(1024)(128)(2,1)S(1)}, bf16[2048]{0:T(1024)(128)(2,1)}, u32[]{:S(2)}) copy-start(bf16[2048]{0:T(1024)(128)(2,1)} %param.21) | copy-start | bytes 12292
  75.9 15.7 %copy-start.6 = (bf16[1,2048,128]{2,1,0:T(8,128)(2,1)S(1)}, bf16[1,2048,128]{2,1,0:T(8,128)(2,1)}, u32[]{:S(2)}) copy-start(bf16[1,2048,128]{2,1,0:T(8,128)(2,1)} %w_ref.3) | copy-start | bytes 1572868

commit v4 on v3

--- a/solution.py
+++ b/solution.py
@@ -21,7 +21,6 @@
 BF16 = jnp.bfloat16
 VM = pl.BlockSpec(memory_space=pltpu.VMEM)
 HB = pl.BlockSpec(memory_space=pltpu.HBM)
-SM = pl.BlockSpec(memory_space=pltpu.SMEM)
 
 
 def call(body, outs, operands, specs, scratch=(), flops=1_000_000, moved=1_000_000, limit=VMEM_LIMIT):
@@ -40,12 +39,15 @@
     return jax.ShapeDtypeStruct(shape, dtype)
 
 
+def own_place():
+    return lax.axis_index("y") * CORES + lax.axis_index("core")
+
+
 def held(shape, dtype):
     return pltpu.VMEM(shape, dtype)
 
 
 def head_kernel(
-    place_ref,
     length_hbm,
     tokens_hbm,
     gain_hbm,
@@ -100,7 +102,8 @@
         axis=1,
     )
     normed_ref[...] = normed
-    first = pl.multiple_of(place_ref[0] * lanes, lanes)
+    place = own_place()
+    first = pl.multiple_of(place * lanes, lanes)
     residual_ref[...] = tokens_ref[:, pl.ds(first, lanes)]
     for load in loads[2:]:
         load.wait()
@@ -143,7 +146,6 @@
 
 
 def attend_kernel(
-    place_ref,
     used_ref,
     query_ref,
     normed_ref,
@@ -155,8 +157,9 @@
     values_ref,
     cum_ref,
     out_ref,
+    rows_ref,
 ):
-    place = place_ref[0]
+    place = own_place()
     normed = normed_ref[...]
     rows = normed.shape[0]
     own_row = lax.broadcasted_iota(jnp.int32, (rows, 1), 0) == place
@@ -182,9 +185,10 @@
     def index(shape, dim):
         return lax.broadcasted_iota(jnp.int32, shape, dim)
 
-    to_heads = (index((heads, pairs), 0) // 2 == index((heads, pairs), 1)).astype(BF16)
-    to_pairs = (index((pairs, heads), 1) // 2 == index((pairs, heads), 0)).astype(BF16)
-    doubled = jnp.dot(to_heads, query_ref[...], preferred_element_type=F32)
+    query = query_ref[...].astype(F32)
+    rows_ref[pl.ds(0, pairs, stride=2), :] = query
+    rows_ref[pl.ds(1, pairs, stride=2), :] = query
+    doubled = rows_ref[...]
     odd_row = index((heads, HEAD), 0) % 2 == 1
     one_head = jnp.where(odd_row, doubled[:, HEAD:], doubled[:, :HEAD])
     in_block = index((heads, width), 1) // HEAD == index((heads, width), 0) // (heads // KV_HEADS)
@@ -209,10 +213,10 @@
     summed = jnp.where(in_block, summed, 0.0)
     summed = summed[:, : 2 * HEAD] + summed[:, 2 * HEAD :]
     summed = (summed[:, :HEAD] + summed[:, HEAD:]) / denominator
-    both = jnp.concatenate([summed, summed], axis=1).astype(BF16)
-    mine = index(both.shape, 1) // HEAD == index(both.shape, 0) % 2
-    both = jnp.where(mine, both, jnp.zeros((), BF16))
-    attended = jnp.dot(to_pairs, both, preferred_element_type=F32).astype(BF16)
+    rows_ref[...] = jnp.concatenate([summed, summed], axis=1)
+    even = rows_ref[pl.ds(0, pairs, stride=2), :]
+    odd = rows_ref[pl.ds(1, pairs, stride=2), :]
+    attended = jnp.where(index((pairs, 2 * HEAD), 1) < HEAD, even, odd).astype(BF16)
     out_ref[...] = jnp.broadcast_to(attended[None], out_ref.shape)
 
 
@@ -251,11 +255,12 @@
 
 
 def down_kernel(parts_ref, w_ref, out_ref, hidden_ref):
-    cores, chips, _, lanes = parts_ref.shape
+    cores, peers, rows, lanes = parts_ref.shape
     for core in range(cores):
-        for chip in range(chips):
-            first = (chip * cores + core) * lanes
-            hidden_ref[:, first : first + lanes] = parts_ref[core, chip]
+        for peer in range(peers):
+            hidden_ref[core * rows : (core + 1) * rows, peer * lanes : (peer + 1) * lanes] = parts_ref[
+                core, peer
+            ]
     out_ref[...] = jnp.dot(hidden_ref[...], w_ref[0], preferred_element_type=F32).astype(BF16)
 
 
@@ -281,6 +286,12 @@
 
     def to_all(copies):
         exchanged = lax.all_to_all(copies, "y", 0, 0, tiled=True)
+        return lax.all_gather(exchanged, "core", axis=0, tiled=False)
+
+    def halves_to_all(copies):
+        rows, lanes = copies.shape[1:]
+        halves = copies.reshape(peers, rows // CORES, lanes)
+        exchanged = lax.all_to_all(halves, tp, 0, 0, tiled=True)
         return lax.all_gather(exchanged, "core", axis=0, tiled=False)
 
     def on_device(
@@ -307,8 +318,6 @@
         rows, features = tokens.shape
         part = w_query.shape[1]
         slots = experts * TOP
-        place = (lax.axis_index("y") * CORES + lax.axis_index("core")).astype(jnp.int32)
-        place = place.reshape(1)
         def head(*refs):
             head_kernel(*refs, per_group=experts // GROUPS)
 
@@ -333,8 +342,8 @@
                 held((8, 128), jnp.int32),
                 held((rows, part), BF16),
             ),
-            (place, *operands),
-            [SM] + [HB] * len(operands),
+            operands,
+            [HB] * len(operands),
             scratch=[pltpu.VMEM(one.shape, one.dtype) for one in operands]
             + [pltpu.SemaphoreType.DMA((len(operands),))],
             flops=10_000_000,
@@ -354,7 +363,6 @@
             attend_kernel,
             shaped((peers, peers, part), BF16),
             (
-                place,
                 used,
                 own_query,
                 normed,
@@ -366,7 +374,8 @@
                 cache_values,
                 cache_logcum,
             ),
-            [SM] + [VM] * 10,
+            [VM] * 10,
+            scratch=[pltpu.VMEM((QUERY_HEAD_COUNT, 2 * HEAD), F32)],
             flops=200_000_000,
         )
         attended = lax.all_to_all(copies, tp, 0, 0, tiled=True)
@@ -392,7 +401,7 @@
         result = call(
             down_kernel,
             shaped((slots, part), BF16),
-            (to_all(hidden), w_down),
+            (halves_to_all(hidden), w_down),
             [VM] * 2,
             scratch=[pltpu.VMEM((slots, features), BF16)],
             flops=50_000_000,

time: 108 us -> 107 us (level)
    all_to_all x0 -> x1, blocking collectives: none -> 13.2 us  [halves_to_all(): exchanged = lax.all_to_all(halves, tp, 0, 0, tiled=True)]
    all_to_all x2 -> x1, blocking collectives: 23.6 us -> 11.1 us  [to_all(): exchanged = lax.all_to_all(copies, 'y', 0, 0, tiled=True)]
    all_gather x2 -> x1, blocking collectives: 7.83 us -> 4.71 us  [to_all(): return lax.all_gather(exchanged, 'core', axis=0, tiled=False)]
    all_gather x0 -> x1, blocking collectives: none -> 2.08 us  [halves_to_all(): return lax.all_gather(exchanged, 'core', axis=0, tiled=False)]
where the time goes in v4:
time: 107 us
  blocking collectives  101 us (94%)
  Pallas kernels  4.71 us (4%)
    all_to_all x1, blocking collectives, on_device(): lax.all_to_all(packed.reshape(experts, TOP, part), 'ep', 0, 0, tiled=True)  24.3 us
    all_to_all x1, blocking collectives, on_device(): lax.all_to_all(query.reshape(peers, 1, part), tp, split_axis=0, concat_ax...  20.2 us
    all_to_all x1, blocking collectives, on_device(): lax.all_to_all(result.reshape(experts, TOP, part), 'ep', 0, 0, tiled=True)  14.7 us
    all_to_all x1, blocking collectives, halves_to_all(): exchanged = lax.all_to_all(halves, tp, 0, 0, tiled=True)  13.2 us
    all_to_all x1, blocking collectives, to_all(): exchanged = lax.all_to_all(copies, 'y', 0, 0, tiled=True)  11.1 us
    all_to_all x1, blocking collectives, on_device(): attended = lax.all_to_all(copies, tp, 0, 0, tiled=True)  10.9 us
    pallas_call x7, Pallas kernels, call(): pl.pallas_call(body, out_shape=outs, in_specs=specs, out_specs=jax.tree.m...  4.71 us
    all_gather x1, blocking collectives, to_all(): return lax.all_gather(exchanged, 'core', axis=0, tiled=False)  4.71 us

profile of v4, /device:TPU:1, one launch (start us, length us, event | category | flops | bytes accessed | tf_op | source)
XLA Modules:
  0.0 106.8 jit_solution(16589079393477677314)
XLA Ops:
  0.7 1.4 %shard_map.181 = (bf16[16,128]{1,0:T(8,128)(2,1)S(1)}, bf16[16,2048]{1,0:T(8,128)(2,1)S(1)}, f32[32,128]{1,0:T(8,128)S(1)}, bf16[96,16]{1,0:T(8,128)(2,1)S(1)}, ...) custom-call(s32[1,1]{1,0:T(1,128)} %bitcast.19.refs_0_, bf16[16,2048]{1,0:T(8,128)(2,1)} %refs_1_.1, ...), custom_call_target="tpu_custom_call" | custom-call | flops 10000000 | bytes 1000000 | tf_op jit(solution)/shard_map/pallas_call | solution.py:27
  2.0 0.0 copy-start
  2.0 0.0 copy-start.1
  2.1 0.0 copy-start.2
  2.1 0.0 copy-start.3
  2.1 0.0 copy-start.8
  2.1 0.0 copy-start.9
  2.1 20.2 %all_to_all.30 = bf16[16,1,128]{2,1,0:T(2,128)(2,1)S(1)} all-to-all(bf16[16,1,128]{2,1,0:T(2,128)(2,1)S(1)} %copy.21), channel_id=1, replica_groups=mesh['ep'=48,'y'=8,'core'=2] {'y','core'}, dimensions={0} | all-to-all | bytes 8192 | tf_op jit(solution)/shard_map/all_to_all | solution.py:359
  22.3 0.0 copy-done
  22.4 0.0 copy-done.1
  22.4 0.0 copy-done.2
  22.4 0.0 copy-done.3
  22.4 0.0 copy-done.8
  22.4 0.0 copy-done.9
  22.4 0.0 copy-start.7
  22.4 1.5 %shard_map.183 = bf16[16,16,128]{2,1,0:T(8,128)(2,1)S(1)} custom-call(s32[8,128]{1,0:T(8,128)S(1)} %get-tuple-element.14.used_ref, bf16[16,128]{1,0:T(8,128)(2,1)S(1)} %bitcast.27, bf16[16,2048]{1,0:T(8,128)(2,1)S(1)} %get-tuple-element.16.normed_ref, bf16[2048,256]{1,0:T(8,128)(2,1)S(1)} %copy-done, bf16[2048,256]{1,0:T(8,128)(2,1)S(1)} %copy-done.1, ...), custom_call_target="tpu_custom_call" | custom-call | flops 200000000 | bytes 1000000 | tf_op jit(solution)/shard_map/pallas_call | solution.py:27
  23.9 10.9 %all_to_all.31.parts_ref = bf16[16,16,128]{2,1,0:T(8,128)(2,1)S(1)} all-to-all(bf16[16,16,128]{2,1,0:T(8,128)(2,1)S(1)} %shard_map.183), channel_id=1, replica_groups=mesh['ep'=48,'y'=8,'core'=2] {'y','core'}, dimensions={0} | all-to-all | bytes 131072 | tf_op jit(solution)/shard_map/all_to_all | solution.py:381
  34.8 0.0 copy-done.7
  34.8 0.3 shard_map.184
  35.1 24.3 %all_to_all.32 = bf16[48,2,128]{2,1,0:T(2,128)(2,1)S(1)} all-to-all(bf16[48,2,128]{2,1,0:T(2,128)(2,1)S(1)} %bitcast.26), channel_id=1, replica_groups=mesh['ep'=48,'y'=8,'core'=2] {'ep'}, dimensions={0} | all-to-all | bytes 49152 | tf_op jit(solution)/shard_map/all_to_all | solution.py:390
  59.4 0.0 copy-start.4
  59.4 11.1 %all_to_all.33 = bf16[8,96,128]{2,1,0:T(8,128)(2,1)S(1)} all-to-all(bf16[8,96,128]{2,1,0:T(8,128)(2,1)S(1)} %broadcast_in_dim.8), channel_id=1, replica_groups=mesh['ep'=48,'y'=8,'core'=2] {'y'}, dimensions={0} | all-to-all | bytes 393216 | tf_op jit(solution)/shard_map/all_to_all | solution.py:288
  70.5 4.7 %all-gather = bf16[16,96,128]{2,1,0:T(8,128)(2,1)S(1)} all-gather(bf16[8,96,128]{2,1,0:T(8,128)(2,1)S(1)} %all_to_all.33), channel_id=2, replica_groups=mesh['ep'=48,'y'=8,'core'=2] {'core'}, dimensions={0}, use_global_device_ids=true | all-gather | bytes 589824 | tf_op jit(solution)/shard_map/all_gather | solution.py:289
  75.2 0.0 copy-done.5
  75.2 0.0 copy-done.4
  75.2 0.5 shard_map.185
  75.7 0.0 copy-start.6
  75.7 13.2 %all_to_all.34 = bf16[16,48,128]{2,1,0:T(8,128)(2,1)S(1)} all-to-all(bf16[16,48,128]{2,1,0:T(8,128)(2,1)S(1)} %bitcast.22), channel_id=1, replica_groups=mesh['ep'=48,'y'=8,'core'=2] {'y','core'}, dimensions={0} | all-to-all | bytes 393216 | tf_op jit(solution)/shard_map/all_to_all | solution.py:294
  88.9 2.1 %all-gather.1 = bf16[32,48,128]{2,1,0:T(8,128)(2,1)S(1)} all-gather(bf16[16,48,128]{2,1,0:T(8,128)(2,1)S(1)} %all_to_all.34), channel_id=3, replica_groups=mesh['ep'=48,'y'=8,'core'=2] {'core'}, dimensions={0}, use_global_device_ids=true | all-gather | bytes 589824 | tf_op jit(solution)/shard_map/all_gather | solution.py:295
  91.0 0.3 shard_map.186
  91.3 14.7 %all_to_all.35 = bf16[48,2,128]{2,1,0:T(2,128)(2,1)S(1)} all-to-all(bf16[48,2,128]{2,1,0:T(2,128)(2,1)S(1)} %bitcast.25), channel_id=1, replica_groups=mesh['ep'=48,'y'=8,'core'=2] {'ep'}, dimensions={0} | all-to-all | bytes 49152 | tf_op jit(solution)/shard_map/all_to_all | solution.py:409
  106.0 0.8 shard_map.187
  (8 shorter events, 0.0 us)
Async XLA Ops:
  2.0 20.3 %copy-start = (bf16[2048,256]{1,0:T(8,128)(2,1)S(1)}, bf16[2048,256]{1,0:T(8,128)(2,1)}, u32[]{:S(2)}) copy-start(bf16[2048,256]{1,0:T(8,128)(2,1)} %w_key_ref.1) | copy-start | bytes 3145732
  2.0 20.3 %copy-start.1 = (bf16[2048,256]{1,0:T(8,128)(2,1)S(1)}, bf16[2048,256]{1,0:T(8,128)(2,1)}, u32[]{:S(2)}) copy-start(bf16[2048,256]{1,0:T(8,128)(2,1)} %w_value_ref.1) | copy-start | bytes 3145732
  2.1 20.3 %copy-start.2 = (bf16[1,2048,256]{2,1,0:T(8,128)(2,1)S(1)}, bf16[1,2048,256]{2,1,0:T(8,128)(2,1)}, u32[]{:S(2)}) copy-start(bf16[1,2048,256]{2,1,0:T(8,128)(2,1)} %keys_ref.1) | copy-start | bytes 3145732
  2.1 20.3 %copy-start.3 = (bf16[1,2048,256]{2,1,0:T(8,128)(2,1)S(1)}, bf16[1,2048,256]{2,1,0:T(8,128)(2,1)}, u32[]{:S(2)}) copy-start(bf16[1,2048,256]{2,1,0:T(8,128)(2,1)} %values_ref.1) | copy-start | bytes 3145732
  2.1 20.3 %copy-start.8 = (f32[1,32,2048]{2,1,0:T(8,128)S(1)}, f32[1,32,2048]{2,1,0:T(8,128)}, u32[]{:S(2)}) copy-start(f32[1,32,2048]{2,1,0:T(8,128)} %cum_ref.1) | copy-start | bytes 786436
  2.1 20.3 %copy-start.9 = (bf16[2048,32]{0,1:T(8,128)(2,1)S(1)}, bf16[2048,32]{0,1:T(8,128)(2,1)}, u32[]{:S(2)}) copy-start(bf16[2048,32]{0,1:T(8,128)(2,1)} %param.25) | copy-start | bytes 393220
  22.4 12.4 %copy-start.7 = (bf16[2048,128]{1,0:T(8,128)(2,1)S(1)}, bf16[2048,128]{1,0:T(8,128)(2,1)}, u32[]{:S(2)}) copy-start(bf16[2048,128]{1,0:T(8,128)(2,1)} %w_ref.2) | copy-start | bytes 1572868
  59.3 15.9 %copy-start.5 = (bf16[1,2048,128]{2,1,0:T(8,128)(2,1)S(1)}, bf16[1,2048,128]{2,1,0:T(8,128)(2,1)}, u32[]{:S(2)}) copy-start(bf16[1,2048,128]{2,1,0:T(8,128)(2,1)} %w_up_ref.1) | copy-start | bytes 1572868
  59.4 15.8 %copy-start.4 = (bf16[1,2048,128]{2,1,0:T(8,128)(2,1)S(1)}, bf16[1,2048,128]{2,1,0:T(8,128)(2,1)}, u32[]{:S(2)}) copy-start(bf16[1,2048,128]{2,1,0:T(8,128)(2,1)} %w_gate_ref.1) | copy-start | bytes 1572868
  70.5 4.7 %copy-start.10 = (bf16[2048]{0:T(1024)(128)(2,1)S(1)}, bf16[2048]{0:T(1024)(128)(2,1)}, u32[]{:S(2)}) copy-start(bf16[2048]{0:T(1024)(128)(2,1)} %param.21) | copy-start | bytes 12292
  75.7 15.3 %copy-start.6 = (bf16[1,2048,128]{2,1,0:T(8,128)(2,1)S(1)}, bf16[1,2048,128]{2,1,0:T(8,128)(2,1)}, u32[]{:S(2)}) copy-start(bf16[1,2048,128]{2,1,0:T(8,128)(2,1)} %w_ref.3) | copy-start | bytes 1572868

commit v5 on v4

--- a/solution.py
+++ b/solution.py
@@ -113,6 +113,8 @@
     row_index = lax.broadcasted_iota(jnp.int32, (rows, rows), 0)
     column_index = lax.broadcasted_iota(jnp.int32, (rows, rows), 1)
     lines = [picked[j : j + 1] for j in range(TOP)]
+    half = send_ref.shape[0] // TOP // 2
+    in_order = [jnp.where(line < half, line + half, line - half) for line in lines]
     columns = [
         jnp.sum(jnp.where(row_index == column_index, line, 0), axis=1, keepdims=True)
         for line in lines
@@ -126,7 +128,7 @@
         for other in columns:
             same = (other == lines[j]) & (row_index < column_index)
             earlier = earlier + jnp.sum(same.astype(jnp.int32), axis=0, keepdims=True)
-        hit = slot_index == lines[j] * TOP + earlier
+        hit = slot_index == in_order[j] * TOP + earlier
         send = send + jnp.where(hit, 1.0, 0.0)
         combine = combine + jnp.where(hit, weight_ref[j : j + 1], 0.0)
     send_ref[...] = send.astype(BF16)
@@ -255,12 +257,11 @@
 
 
 def down_kernel(parts_ref, w_ref, out_ref, hidden_ref):
-    cores, peers, rows, lanes = parts_ref.shape
+    cores, chips, _, lanes = parts_ref.shape
     for core in range(cores):
-        for peer in range(peers):
-            hidden_ref[core * rows : (core + 1) * rows, peer * lanes : (peer + 1) * lanes] = parts_ref[
-                core, peer
-            ]
+        for i in range(chips):
+            first = ((chips - 1 - i) * cores + core) * lanes
+            hidden_ref[:, first : first + lanes] = parts_ref[core, i]
     out_ref[...] = jnp.dot(hidden_ref[...], w_ref[0], preferred_element_type=F32).astype(BF16)
 
 
@@ -284,15 +285,16 @@
     split = Mesh(mesh.devices.reshape(experts, chips, CORES), ("ep", "y", "core"))
     tp = ("y", "core")
 
-    def to_all(copies):
-        exchanged = lax.all_to_all(copies, "y", 0, 0, tiled=True)
+    def to_all(copies, order=None):
+        groups = None if order is None else [order]
+        exchanged = lax.all_to_all(copies, "y", 0, 0, tiled=True, axis_index_groups=groups)
         return lax.all_gather(exchanged, "core", axis=0, tiled=False)
 
-    def halves_to_all(copies):
-        rows, lanes = copies.shape[1:]
-        halves = copies.reshape(peers, rows // CORES, lanes)
-        exchanged = lax.all_to_all(halves, tp, 0, 0, tiled=True)
-        return lax.all_gather(exchanged, "core", axis=0, tiled=False)
+    chip_order = list(range(chips))[::-1]
+    expert_order = [(i + experts // 2) % experts for i in range(experts)]
+
+    def over_experts(rows):
+        return lax.all_to_all(rows, "ep", 0, 0, tiled=True, axis_index_groups=[expert_order])
 
     def on_device(
         tokens,
@@ -387,7 +389,7 @@
             scratch=[pltpu.VMEM((rows * peers, part), F32)],
             flops=20_000_000,
         )
-        arrived = lax.all_to_all(packed.reshape(experts, TOP, part), "ep", 0, 0, tiled=True)
+        arrived = over_experts(packed.reshape(experts, TOP, part))
         arrived = arrived.reshape(slots, part)
         parts = to_all(jnp.broadcast_to(arrived[None], (chips, slots, part)))
         hidden = call(
@@ -401,12 +403,12 @@
         result = call(
             down_kernel,
             shaped((slots, part), BF16),
-            (halves_to_all(hidden), w_down),
+            (to_all(hidden, chip_order), w_down),
             [VM] * 2,
             scratch=[pltpu.VMEM((slots, features), BF16)],
             flops=50_000_000,
         )
-        returned = lax.all_to_all(result.reshape(experts, TOP, part), "ep", 0, 0, tiled=True)
+        returned = over_experts(result.reshape(experts, TOP, part))
         return call(
             combine_kernel,
             shaped((rows, part), BF16),

time: 107 us -> 103 us (0.963)
  blocking collectives: 101 us -> 96.5 us
    all_to_all x4, blocking collectives: 63.3 us -> 57 us  [the longest x2 36.4 us: over_experts(): lax.all_to_all(rows, 'ep', 0, 0, tiled=True, axis_index_groups=[expert_or...]
    all_gather x1 -> x2, blocking collectives: 4.71 us -> 8.43 us  [to_all(): return lax.all_gather(exchanged, 'core', axis=0, tiled=False)]
    all_gather x1 -> x0, blocking collectives: 2.08 us -> none  [halves_to_all(): return lax.all_gather(exchanged, 'core', axis=0, tiled=False)]
where the time goes in v5:
time: 103 us; the launch traced here: 102 us
  blocking collectives  96.5 us (94%)
  Pallas kernels  4.71 us (5%)
    all_to_all x2, blocking collectives, over_experts(): lax.all_to_all(rows, 'ep', 0, 0, tiled=True, axis_index_groups=[expert_or...  36.4 us
    all_to_all x2, blocking collectives, to_all(): lax.all_to_all(copies, 'y', 0, 0, tiled=True, axis_index_groups=groups)  20.5 us
    all_to_all x1, blocking collectives, on_device(): lax.all_to_all(query.reshape(peers, 1, part), tp, split_axis=0, concat_ax...  20.2 us
    all_to_all x1, blocking collectives, on_device(): attended = lax.all_to_all(copies, tp, 0, 0, tiled=True)  10.9 us
    all_gather x2, blocking collectives, to_all(): return lax.all_gather(exchanged, 'core', axis=0, tiled=False)  8.43 us
    pallas_call x7, Pallas kernels, call(): pl.pallas_call(body, out_shape=outs, in_specs=specs, out_specs=jax.tree.m...  4.71 us

profile of v5, /device:TPU:1, one launch (start us, length us, event | category | flops | bytes accessed | tf_op | source)
XLA Modules:
  0.0 102.1 jit_solution(18430939038180949937)
XLA Ops:
  0.7 1.4 %shard_map.181 = (bf16[16,128]{1,0:T(8,128)(2,1)S(1)}, bf16[16,2048]{1,0:T(8,128)(2,1)S(1)}, f32[32,128]{1,0:T(8,128)S(1)}, bf16[96,16]{1,0:T(8,128)(2,1)S(1)}, ...) custom-call(s32[1,1]{1,0:T(1,128)} %bitcast.18.refs_0_, bf16[16,2048]{1,0:T(8,128)(2,1)} %refs_1_.1, ...), custom_call_target="tpu_custom_call" | custom-call | flops 10000000 | bytes 1000000 | tf_op jit(solution)/shard_map/pallas_call | solution.py:27
  2.0 0.0 copy-start
  2.0 0.0 copy-start.1
  2.1 0.0 copy-start.2
  2.1 0.0 copy-start.3
  2.1 0.0 copy-start.8
  2.1 0.0 copy-start.9
  2.1 20.2 %all_to_all.30 = bf16[16,1,128]{2,1,0:T(2,128)(2,1)S(1)} all-to-all(bf16[16,1,128]{2,1,0:T(2,128)(2,1)S(1)} %copy.21), channel_id=1, replica_groups=mesh['ep'=48,'y'=8,'core'=2] {'y','core'}, dimensions={0} | all-to-all | bytes 8192 | tf_op jit(solution)/shard_map/all_to_all | solution.py:361
  22.3 0.0 copy-done
  22.4 0.0 copy-done.1
  22.4 0.0 copy-done.2
  22.4 0.0 copy-done.3
  22.4 0.0 copy-done.8
  22.4 0.0 copy-done.9
  22.4 0.0 copy-start.7
  22.4 1.5 %shard_map.183 = bf16[16,16,128]{2,1,0:T(8,128)(2,1)S(1)} custom-call(s32[8,128]{1,0:T(8,128)S(1)} %get-tuple-element.14.used_ref, bf16[16,128]{1,0:T(8,128)(2,1)S(1)} %bitcast.25, bf16[16,2048]{1,0:T(8,128)(2,1)S(1)} %get-tuple-element.16.normed_ref, bf16[2048,256]{1,0:T(8,128)(2,1)S(1)} %copy-done, bf16[2048,256]{1,0:T(8,128)(2,1)S(1)} %copy-done.1, ...), custom_call_target="tpu_custom_call" | custom-call | flops 200000000 | bytes 1000000 | tf_op jit(solution)/shard_map/pallas_call | solution.py:27
  23.9 10.9 %all_to_all.31.parts_ref = bf16[16,16,128]{2,1,0:T(8,128)(2,1)S(1)} all-to-all(bf16[16,16,128]{2,1,0:T(8,128)(2,1)S(1)} %shard_map.183), channel_id=1, replica_groups=mesh['ep'=48,'y'=8,'core'=2] {'y','core'}, dimensions={0} | all-to-all | bytes 131072 | tf_op jit(solution)/shard_map/all_to_all | solution.py:383
  34.8 0.0 copy-done.7
  34.8 0.3 shard_map.184
  35.1 21.8 %all_to_all.32 = bf16[48,2,128]{2,1,0:T(2,128)(2,1)S(1)} all-to-all(bf16[48,2,128]{2,1,0:T(2,128)(2,1)S(1)} %bitcast.24), channel_id=1, replica_groups={{384,400,416,432,448,464,480,496,512,528,544,560,576,592,608,624,640,65..., dimensions={0} | all-to-all | bytes 49152 | tf_op jit(solution)/shard_map/all_to_all | solution.py:297
  56.9 0.0 copy-start.4
  56.9 11.1 %all_to_all.33 = bf16[8,96,128]{2,1,0:T(8,128)(2,1)S(1)} all-to-all(bf16[8,96,128]{2,1,0:T(8,128)(2,1)S(1)} %broadcast_in_dim.8), channel_id=1, replica_groups=mesh['ep'=48,'y'=8,'core'=2] {'y'}, dimensions={0} | all-to-all | bytes 393216 | tf_op jit(solution)/shard_map/all_to_all | solution.py:290
  68.0 4.7 %all-gather = bf16[16,96,128]{2,1,0:T(8,128)(2,1)S(1)} all-gather(bf16[8,96,128]{2,1,0:T(8,128)(2,1)S(1)} %all_to_all.33), channel_id=2, replica_groups=mesh['ep'=48,'y'=8,'core'=2] {'core'}, dimensions={0}, use_global_device_ids=true | all-gather | bytes 589824 | tf_op jit(solution)/shard_map/all_gather | solution.py:291
  72.7 0.0 copy-done.5
  72.7 0.0 copy-done.4
  72.7 0.5 shard_map.185
  73.2 0.0 copy-start.6
  73.2 9.4 %all_to_all.34 = bf16[8,96,128]{2,1,0:T(8,128)(2,1)S(1)} all-to-all(bf16[8,96,128]{2,1,0:T(8,128)(2,1)S(1)} %shard_map.185), channel_id=1, replica_groups={{14,12,10,8,6,4,2,0},{15,13,11,9,7,5,3,1},{30,28,26,24,22,20,18,16},{31..., dimensions={0} | all-to-all | bytes 393216 | tf_op jit(solution)/shard_map/all_to_all | solution.py:290
  82.7 3.7 %all-gather.1 = bf16[16,96,128]{2,1,0:T(8,128)(2,1)S(1)} all-gather(bf16[8,96,128]{2,1,0:T(8,128)(2,1)S(1)} %all_to_all.34), channel_id=3, replica_groups=mesh['ep'=48,'y'=8,'core'=2] {'core'}, dimensions={0}, use_global_device_ids=true | all-gather | bytes 589824 | tf_op jit(solution)/shard_map/all_gather | solution.py:291
  86.4 0.3 shard_map.186
  86.7 14.6 %all_to_all.35 = bf16[48,2,128]{2,1,0:T(2,128)(2,1)S(1)} all-to-all(bf16[48,2,128]{2,1,0:T(2,128)(2,1)S(1)} %bitcast.23), channel_id=1, replica_groups={{384,400,416,432,448,464,480,496,512,528,544,560,576,592,608,624,640,65..., dimensions={0} | all-to-all | bytes 49152 | tf_op jit(solution)/shard_map/all_to_all | solution.py:297
  101.3 0.8 shard_map.187
  (8 shorter events, 0.0 us)
Async XLA Ops:
  2.0 20.3 %copy-start = (bf16[2048,256]{1,0:T(8,128)(2,1)S(1)}, bf16[2048,256]{1,0:T(8,128)(2,1)}, u32[]{:S(2)}) copy-start(bf16[2048,256]{1,0:T(8,128)(2,1)} %w_key_ref.1) | copy-start | bytes 3145732
  2.0 20.3 %copy-start.1 = (bf16[2048,256]{1,0:T(8,128)(2,1)S(1)}, bf16[2048,256]{1,0:T(8,128)(2,1)}, u32[]{:S(2)}) copy-start(bf16[2048,256]{1,0:T(8,128)(2,1)} %w_value_ref.1) | copy-start | bytes 3145732
  2.1 20.3 %copy-start.2 = (bf16[1,2048,256]{2,1,0:T(8,128)(2,1)S(1)}, bf16[1,2048,256]{2,1,0:T(8,128)(2,1)}, u32[]{:S(2)}) copy-start(bf16[1,2048,256]{2,1,0:T(8,128)(2,1)} %keys_ref.1) | copy-start | bytes 3145732
  2.1 20.3 %copy-start.3 = (bf16[1,2048,256]{2,1,0:T(8,128)(2,1)S(1)}, bf16[1,2048,256]{2,1,0:T(8,128)(2,1)}, u32[]{:S(2)}) copy-start(bf16[1,2048,256]{2,1,0:T(8,128)(2,1)} %values_ref.1) | copy-start | bytes 3145732
  2.1 20.3 %copy-start.8 = (f32[1,32,2048]{2,1,0:T(8,128)S(1)}, f32[1,32,2048]{2,1,0:T(8,128)}, u32[]{:S(2)}) copy-start(f32[1,32,2048]{2,1,0:T(8,128)} %cum_ref.1) | copy-start | bytes 786436
  2.1 20.3 %copy-start.9 = (bf16[2048,32]{0,1:T(8,128)(2,1)S(1)}, bf16[2048,32]{0,1:T(8,128)(2,1)}, u32[]{:S(2)}) copy-start(bf16[2048,32]{0,1:T(8,128)(2,1)} %param.25) | copy-start | bytes 393220
  22.4 12.4 %copy-start.7 = (bf16[2048,128]{1,0:T(8,128)(2,1)S(1)}, bf16[2048,128]{1,0:T(8,128)(2,1)}, u32[]{:S(2)}) copy-start(bf16[2048,128]{1,0:T(8,128)(2,1)} %w_ref.2) | copy-start | bytes 1572868
  56.8 15.9 %copy-start.5 = (bf16[1,2048,128]{2,1,0:T(8,128)(2,1)S(1)}, bf16[1,2048,128]{2,1,0:T(8,128)(2,1)}, u32[]{:S(2)}) copy-start(bf16[1,2048,128]{2,1,0:T(8,128)(2,1)} %w_up_ref.1) | copy-start | bytes 1572868
  56.9 15.8 %copy-start.4 = (bf16[1,2048,128]{2,1,0:T(8,128)(2,1)S(1)}, bf16[1,2048,128]{2,1,0:T(8,128)(2,1)}, u32[]{:S(2)}) copy-start(bf16[1,2048,128]{2,1,0:T(8,128)(2,1)} %w_gate_ref.1) | copy-start | bytes 1572868
  68.0 4.7 %copy-start.10 = (bf16[2048]{0:T(1024)(128)(2,1)S(1)}, bf16[2048]{0:T(1024)(128)(2,1)}, u32[]{:S(2)}) copy-start(bf16[2048]{0:T(1024)(128)(2,1)} %param.21) | copy-start | bytes 12292
  73.2 13.2 %copy-start.6 = (bf16[1,2048,128]{2,1,0:T(8,128)(2,1)S(1)}, bf16[1,2048,128]{2,1,0:T(8,128)(2,1)}, u32[]{:S(2)}) copy-start(bf16[1,2048,128]{2,1,0:T(8,128)(2,1)} %w_ref.3) | copy-start | bytes 1572868

commit v6 on v5

--- a/solution.py
+++ b/solution.py
@@ -74,6 +74,7 @@
     sems,
     *,
     per_group,
+    first_expert,
 ):
     sources = (
         tokens_hbm, gain_hbm, w_query_hbm, group_hbm, expert_hbm, weight_hbm, bias_hbm, length_hbm
@@ -113,8 +114,11 @@
     row_index = lax.broadcasted_iota(jnp.int32, (rows, rows), 0)
     column_index = lax.broadcasted_iota(jnp.int32, (rows, rows), 1)
     lines = [picked[j : j + 1] for j in range(TOP)]
-    half = send_ref.shape[0] // TOP // 2
-    in_order = [jnp.where(line < half, line + half, line - half) for line in lines]
+    count = send_ref.shape[0] // TOP
+    in_order = [
+        jnp.where(line < first_expert, line + (count - first_expert), line - first_expert)
+        for line in lines
+    ]
     columns = [
         jnp.sum(jnp.where(row_index == column_index, line, 0), axis=1, keepdims=True)
         for line in lines
@@ -256,11 +260,11 @@
     out_ref[...] = jnp.broadcast_to(hidden[None], out_ref.shape)
 
 
-def down_kernel(parts_ref, w_ref, out_ref, hidden_ref):
-    cores, chips, _, lanes = parts_ref.shape
+def down_kernel(parts_ref, w_ref, out_ref, hidden_ref, *, chip_order):
+    cores, _, _, lanes = parts_ref.shape
     for core in range(cores):
-        for i in range(chips):
-            first = ((chips - 1 - i) * cores + core) * lanes
+        for i, chip in enumerate(chip_order):
+            first = (chip * cores + core) * lanes
             hidden_ref[:, first : first + lanes] = parts_ref[core, i]
     out_ref[...] = jnp.dot(hidden_ref[...], w_ref[0], preferred_element_type=F32).astype(BF16)
 
@@ -290,8 +294,9 @@
         exchanged = lax.all_to_all(copies, "y", 0, 0, tiled=True, axis_index_groups=groups)
         return lax.all_gather(exchanged, "core", axis=0, tiled=False)
 
-    chip_order = list(range(chips))[::-1]
-    expert_order = [(i + experts // 2) % experts for i in range(experts)]
+    chip_order = [*range(chips - 2, -1, -1), chips - 1]
+    first_expert = experts * 7 // 12
+    expert_order = [(i + first_expert) % experts for i in range(experts)]
 
     def over_experts(rows):
         return lax.all_to_all(rows, "ep", 0, 0, tiled=True, axis_index_groups=[expert_order])
@@ -321,7 +326,7 @@
         part = w_query.shape[1]
         slots = experts * TOP
         def head(*refs):
-            head_kernel(*refs, per_group=experts // GROUPS)
+            head_kernel(*refs, per_group=experts // GROUPS, first_expert=first_expert)
 
         operands = (
             cache_len.reshape(1, 1),
@@ -400,8 +405,11 @@
             scratch=[pltpu.VMEM((slots, features), BF16)],
             flops=100_000_000,
         )
+        def down(*refs):
+            down_kernel(*refs, chip_order=chip_order)
+
         result = call(
-            down_kernel,
+            down,
             shaped((slots, part), BF16),
             (to_all(hidden, chip_order), w_down),
             [VM] * 2,

time: 103 us -> 103 us (level)
  no operation moved by 1% of the time
where the time goes in v6:
time: 103 us; the launch traced here: 102 us
  blocking collectives  96.8 us (94%)
  Pallas kernels  4.71 us (5%)
    all_to_all x2, blocking collectives, over_experts(): lax.all_to_all(rows, 'ep', 0, 0, tiled=True, axis_index_groups=[expert_or...  36.3 us
    all_to_all x2, blocking collectives, to_all(): lax.all_to_all(copies, 'y', 0, 0, tiled=True, axis_index_groups=groups)  20.7 us
    all_to_all x1, blocking collectives, on_device(): lax.all_to_all(query.reshape(peers, 1, part), tp, split_axis=0, concat_ax...  20.2 us
    all_to_all x1, blocking collectives, on_device(): attended = lax.all_to_all(copies, tp, 0, 0, tiled=True)  10.9 us
    all_gather x2, blocking collectives, to_all(): return lax.all_gather(exchanged, 'core', axis=0, tiled=False)  8.71 us
    pallas_call x7, Pallas kernels, call(): pl.pallas_call(body, out_shape=outs, in_specs=specs, out_specs=jax.tree.m...  4.71 us

profile of v6, /device:TPU:1, one launch (start us, length us, event | category | flops | bytes accessed | tf_op | source)
XLA Modules:
  0.0 102.4 jit_solution(7636125588300099550)
XLA Ops:
  0.7 1.4 %shard_map.181 = (bf16[16,128]{1,0:T(8,128)(2,1)S(1)}, bf16[16,2048]{1,0:T(8,128)(2,1)S(1)}, f32[32,128]{1,0:T(8,128)S(1)}, bf16[96,16]{1,0:T(8,128)(2,1)S(1)}, ...) custom-call(s32[1,1]{1,0:T(1,128)} %bitcast.18.refs_0_, bf16[16,2048]{1,0:T(8,128)(2,1)} %refs_1_.2, ...), custom_call_target="tpu_custom_call" | custom-call | flops 10000000 | bytes 1000000 | tf_op jit(solution)/shard_map/pallas_call | solution.py:27
  2.0 0.0 copy-start
  2.0 0.0 copy-start.1
  2.1 0.0 copy-start.2
  2.1 0.0 copy-start.3
  2.1 0.0 copy-start.8
  2.1 0.0 copy-start.9
  2.1 20.2 %all_to_all.30 = bf16[16,1,128]{2,1,0:T(2,128)(2,1)S(1)} all-to-all(bf16[16,1,128]{2,1,0:T(2,128)(2,1)S(1)} %copy.21), channel_id=1, replica_groups=mesh['ep'=48,'y'=8,'core'=2] {'y','core'}, dimensions={0} | all-to-all | bytes 8192 | tf_op jit(solution)/shard_map/all_to_all | solution.py:366
  22.3 0.0 copy-done
  22.4 0.0 copy-done.1
  22.4 0.0 copy-done.2
  22.4 0.0 copy-done.3
  22.4 0.0 copy-done.8
  22.4 0.0 copy-start.7
  22.4 1.5 %shard_map.183 = bf16[16,16,128]{2,1,0:T(8,128)(2,1)S(1)} custom-call(s32[8,128]{1,0:T(8,128)S(1)} %get-tuple-element.14.used_ref, bf16[16,128]{1,0:T(8,128)(2,1)S(1)} %bitcast.25, bf16[16,2048]{1,0:T(8,128)(2,1)S(1)} %get-tuple-element.16.normed_ref, bf16[2048,256]{1,0:T(8,128)(2,1)S(1)} %copy-done, bf16[2048,256]{1,0:T(8,128)(2,1)S(1)} %copy-done.1, ...), custom_call_target="tpu_custom_call" | custom-call | flops 200000000 | bytes 1000000 | tf_op jit(solution)/shard_map/pallas_call | solution.py:27
  23.9 10.9 %all_to_all.31.parts_ref = bf16[16,16,128]{2,1,0:T(8,128)(2,1)S(1)} all-to-all(bf16[16,16,128]{2,1,0:T(8,128)(2,1)S(1)} %shard_map.183), channel_id=1, replica_groups=mesh['ep'=48,'y'=8,'core'=2] {'y','core'}, dimensions={0} | all-to-all | bytes 131072 | tf_op jit(solution)/shard_map/all_to_all | solution.py:388
  34.8 0.0 copy-done.7
  34.8 0.3 shard_map.184
  35.1 21.6 %all_to_all.32 = bf16[48,2,128]{2,1,0:T(2,128)(2,1)S(1)} all-to-all(bf16[48,2,128]{2,1,0:T(2,128)(2,1)S(1)} %bitcast.24), channel_id=1, replica_groups={{448,464,480,496,512,528,544,560,576,592,608,624,640,656,672,688,704,72..., dimensions={0} | all-to-all | bytes 49152 | tf_op jit(solution)/shard_map/all_to_all | solution.py:302
  56.7 0.0 copy-start.4
  56.8 11.1 %all_to_all.33 = bf16[8,96,128]{2,1,0:T(8,128)(2,1)S(1)} all-to-all(bf16[8,96,128]{2,1,0:T(8,128)(2,1)S(1)} %broadcast_in_dim.8), channel_id=1, replica_groups=mesh['ep'=48,'y'=8,'core'=2] {'y'}, dimensions={0} | all-to-all | bytes 393216 | tf_op jit(solution)/shard_map/all_to_all | solution.py:294
  67.9 4.7 %all-gather = bf16[16,96,128]{2,1,0:T(8,128)(2,1)S(1)} all-gather(bf16[8,96,128]{2,1,0:T(8,128)(2,1)S(1)} %all_to_all.33), channel_id=2, replica_groups=mesh['ep'=48,'y'=8,'core'=2] {'core'}, dimensions={0}, use_global_device_ids=true | all-gather | bytes 589824 | tf_op jit(solution)/shard_map/all_gather | solution.py:295
  72.6 0.0 copy-done.5
  72.6 0.0 copy-done.10
  72.6 0.5 shard_map.185
  73.1 0.0 copy-start.6
  73.1 9.6 %all_to_all.34 = bf16[8,96,128]{2,1,0:T(8,128)(2,1)S(1)} all-to-all(bf16[8,96,128]{2,1,0:T(8,128)(2,1)S(1)} %shard_map.185), channel_id=1, replica_groups={{12,10,8,6,4,2,0,14},{13,11,9,7,5,3,1,15},{28,26,24,22,20,18,16,30},{29..., dimensions={0} | all-to-all | bytes 393216 | tf_op jit(solution)/shard_map/all_to_all | solution.py:294
  82.7 4.0 %all-gather.1 = bf16[16,96,128]{2,1,0:T(8,128)(2,1)S(1)} all-gather(bf16[8,96,128]{2,1,0:T(8,128)(2,1)S(1)} %all_to_all.34), channel_id=3, replica_groups=mesh['ep'=48,'y'=8,'core'=2] {'core'}, dimensions={0}, use_global_device_ids=true | all-gather | bytes 589824 | tf_op jit(solution)/shard_map/all_gather | solution.py:295
  86.7 0.0 copy-done.6
  86.7 0.3 shard_map.186
  87.0 14.6 %all_to_all.35 = bf16[48,2,128]{2,1,0:T(2,128)(2,1)S(1)} all-to-all(bf16[48,2,128]{2,1,0:T(2,128)(2,1)S(1)} %bitcast.23), channel_id=1, replica_groups={{448,464,480,496,512,528,544,560,576,592,608,624,640,656,672,688,704,72..., dimensions={0} | all-to-all | bytes 49152 | tf_op jit(solution)/shard_map/all_to_all | solution.py:302
  101.6 0.8 shard_map.187
  (8 shorter events, 0.0 us)
Async XLA Ops:
  2.0 20.3 %copy-start = (bf16[2048,256]{1,0:T(8,128)(2,1)S(1)}, bf16[2048,256]{1,0:T(8,128)(2,1)}, u32[]{:S(2)}) copy-start(bf16[2048,256]{1,0:T(8,128)(2,1)} %w_key_ref.1) | copy-start | bytes 3145732
  2.0 20.3 %copy-start.1 = (bf16[2048,256]{1,0:T(8,128)(2,1)S(1)}, bf16[2048,256]{1,0:T(8,128)(2,1)}, u32[]{:S(2)}) copy-start(bf16[2048,256]{1,0:T(8,128)(2,1)} %w_value_ref.1) | copy-start | bytes 3145732
  2.1 20.3 %copy-start.2 = (bf16[1,2048,256]{2,1,0:T(8,128)(2,1)S(1)}, bf16[1,2048,256]{2,1,0:T(8,128)(2,1)}, u32[]{:S(2)}) copy-start(bf16[1,2048,256]{2,1,0:T(8,128)(2,1)} %keys_ref.1) | copy-start | bytes 3145732
  2.1 20.3 %copy-start.3 = (bf16[1,2048,256]{2,1,0:T(8,128)(2,1)S(1)}, bf16[1,2048,256]{2,1,0:T(8,128)(2,1)}, u32[]{:S(2)}) copy-start(bf16[1,2048,256]{2,1,0:T(8,128)(2,1)} %values_ref.1) | copy-start | bytes 3145732
  2.1 20.3 %copy-start.8 = (f32[1,32,2048]{2,1,0:T(8,128)S(1)}, f32[1,32,2048]{2,1,0:T(8,128)}, u32[]{:S(2)}) copy-start(f32[1,32,2048]{2,1,0:T(8,128)} %cum_ref.1) | copy-start | bytes 786436
  2.1 20.3 %copy-start.9 = (bf16[2048,32]{0,1:T(8,128)(2,1)S(1)}, bf16[2048,32]{0,1:T(8,128)(2,1)}, u32[]{:S(2)}) copy-start(bf16[2048,32]{0,1:T(8,128)(2,1)} %param.25) | copy-start | bytes 393220
  22.4 12.4 %copy-start.7 = (bf16[2048,128]{1,0:T(8,128)(2,1)S(1)}, bf16[2048,128]{1,0:T(8,128)(2,1)}, u32[]{:S(2)}) copy-start(bf16[2048,128]{1,0:T(8,128)(2,1)} %w_ref.1) | copy-start | bytes 1572868
  56.7 15.9 %copy-start.5 = (bf16[1,2048,128]{2,1,0:T(8,128)(2,1)S(1)}, bf16[1,2048,128]{2,1,0:T(8,128)(2,1)}, u32[]{:S(2)}) copy-start(bf16[1,2048,128]{2,1,0:T(8,128)(2,1)} %w_up_ref.1) | copy-start | bytes 1572868
  56.7 15.8 %copy-start.4 = (bf16[1,2048,128]{2,1,0:T(8,128)(2,1)S(1)}, bf16[1,2048,128]{2,1,0:T(8,128)(2,1)}, u32[]{:S(2)}) copy-start(bf16[1,2048,128]{2,1,0:T(8,128)(2,1)} %w_gate_ref.1) | copy-start | bytes 1572868
  67.8 4.7 %copy-start.10 = (bf16[2048]{0:T(1024)(128)(2,1)S(1)}, bf16[2048]{0:T(1024)(128)(2,1)}, u32[]{:S(2)}) copy-start(bf16[2048]{0:T(1024)(128)(2,1)} %param.21) | copy-start | bytes 12292
  73.1 13.6 %copy-start.6 = (bf16[1,2048,128]{2,1,0:T(8,128)(2,1)S(1)}, bf16[1,2048,128]{2,1,0:T(8,128)(2,1)}, u32[]{:S(2)}) copy-start(bf16[1,2048,128]{2,1,0:T(8,128)(2,1)} %refs_1_.3) | copy-start | bytes 1572868
